TPU v7x, 256 devices: a whole 4x4x8 slice. The times are simulated.
256 devices in a mesh: ep: 64 (over z, x, core), tp: 4 (over y).
Axes of the slice: x: 4, y: 4, z: 8, core: 2. Of those that a mesh axis runs over, the one named last changes fastest.
Arguments:
- mixer_input: bfloat16 [16384, 2048], P('ep'), may hold values from -6 to 6
- mixer_gain: float32 [2048], replicated, may hold values from 0.1 to 8
- query_one: bfloat16 [2048, 512], P(None, 'tp'), may hold values from -0.1875 to 0.1875
- query_two: bfloat16 [2048, 512], P(None, 'tp'), may hold values from -0.1875 to 0.1875
- key_one: bfloat16 [2048, 256], P(None, 'tp'), may hold values from -0.1875 to 0.1875
- key_two: bfloat16 [2048, 256], P(None, 'tp'), may hold values from -0.1875 to 0.1875
- value_weight: bfloat16 [2048, 512], P(None, 'tp'), may hold values from -0.125 to 0.125
- lambdas: float32 [8], P('tp'), may hold values from 0.3 to 0.8
- head_gain: float32 [128], replicated, may hold values from 0.1 to 1.9
- output_weight: bfloat16 [1024, 2048], P('tp'), may hold values from -0.1875 to 0.1875
- expert_input: bfloat16 [32768, 2048], P(('ep', 'tp')), may hold values from -6 to 6
- expert_gain: float32 [2048], replicated, may hold values from 0.1 to 1.9
- routes: int32 [32768, 2], P(('ep', 'tp')), may hold values from 0 to 63, all different within a row; in each aligned block of 128 rows (0 to 127, 128 to 255, ...) at most 5 rows name the same one
- route_weight: float32 [32768, 2], P(('ep', 'tp')), may hold values from 0.2 to 1
- expert_gate: bfloat16 [64, 2048, 1024], P('ep', None, 'tp'), may hold values from -0.125 to 0.125
- expert_up: bfloat16 [64, 2048, 1024], P('ep', None, 'tp'), may hold values from -0.125 to 0.125
- expert_down: bfloat16 [64, 1024, 2048], P('ep', 'tp'), may hold values from -0.1875 to 0.1875
- shared_gate: bfloat16 [2048, 512], P(None, 'tp'), may hold values from -0.125 to 0.125
- shared_up: bfloat16 [2048, 512], P(None, 'tp'), may hold values from -0.125 to 0.125
- shared_down: bfloat16 [512, 2048], P('tp'), may hold values from -0.25 to 0.25
Outputs:
- mixer_output: bfloat16 [16384, 2048], P(('ep', 'tp'))
- expert_output: bfloat16 [32768, 2048], P(('ep', 'tp'))
Inputs may be any that keep to these rules, and one draw needn't show every extreme that they name: `routes`: each row names 2 different experts; in the rows of one device no expert is named by more than 5 rows, and some device names some expert exactly 5 times.
All inputs are finite; a program needn't handle non-finite values.
Results may differ from a plain program's by a relative error of at most 0.014.
The roundings to bfloat16 on the way count: a program that leaves them out, or rounds other values in their place, can miss the bound.
Values may be sent and summed in bfloat16 or wider, within the bound.
A program may use at most 128 MiB of HBM per device.

v0:
```python
import jax
import jax.numpy as jnp
from jax import lax
from jax.sharding import PartitionSpec as P

HEAD = 64


EPS = 1e-06
NEG = -1e30


def partner_2(block, axis, stride):
    count = lax.axis_size(axis)
    route = []
    for low in range(count):
        high = low | 1 << stride
        if high != low and high < count:
            route += [(low, high), (high, low)]
    return lax.ppermute(block, axis, route)


def joined_along(tiles, dim):
    shape = list(tiles.shape[1:])
    shape[dim] *= tiles.shape[0]
    return jnp.moveaxis(tiles, 0, dim).reshape(shape)


def one_gather(arrays, axis, dims):
    flat = jnp.concatenate([a.reshape(-1) for a in arrays])
    lines, at, done = (lax.all_gather(flat, axis), 0, [])
    for a, dim in zip(arrays, dims):
        tiles = lines[:, at : at + a.size].reshape(-1, *a.shape)
        done.append(joined_along(tiles, dim))
        at += a.size
    return tuple(done)


def cut_along(x, dim, peers):
    shape = x.shape
    tiles = x.reshape(*shape[:dim], peers, shape[dim] // peers, *shape[dim + 1 :])
    return jnp.moveaxis(tiles, dim, 0)


def sum_at_owner(x, axis, dim):
    peers = lax.axis_size(axis)
    tiles = lax.all_to_all(cut_along(x, dim, peers), axis, 0, 0, tiled=True)
    return jnp.sum(tiles.astype(jnp.float32), axis=0)


def normalize(activations, scaling):
    values = activations.astype(jnp.float32)
    factor = lax.rsqrt(jnp.mean(values * values, axis=-1, keepdims=True) + EPS)
    return (values * factor * scaling).astype(jnp.bfloat16)


def unchanged(current):
    return current


def attend(running, which_half, query_pair, key_pair, value_rows, query_start, key_start):
    maxima, totals, weighted = running
    span_rows = value_rows.shape[1]
    query_pos = query_start + jnp.arange(span_rows, dtype=jnp.int32)
    key_pos = key_start + jnp.arange(span_rows, dtype=jnp.int32)
    visible = key_pos[None, :] <= query_pos[:, None]
    for map_index in range(2):
        scores = jnp.einsum(
            "kgqd,kjd->kgqj",
            query_pair[map_index],
            key_pair[map_index],
            preferred_element_type=jnp.float32,
        ) * HEAD ** (-0.5)
        scores = jnp.where(visible, scores, NEG)
        earlier = maxima[which_half, map_index]
        latest = jnp.maximum(earlier, jnp.max(scores, axis=-1))
        shrink = jnp.exp(earlier - latest)
        weights = jnp.where(visible, jnp.exp(scores - latest[..., None]), 0.0)
        totals = totals.at[which_half, map_index].set(
            totals[which_half, map_index] * shrink + jnp.sum(weights, axis=-1)
        )
        product = jnp.einsum(
            "kgqj,kjd->kgqd",
            weights.astype(jnp.bfloat16),
            value_rows,
            preferred_element_type=jnp.float32,
        )
        weighted = weighted.at[which_half, map_index].set(
            weighted[which_half, map_index] * shrink[..., None] + product
        )
        maxima = maxima.at[which_half, map_index].set(latest)
    return (maxima, totals, weighted)


def body(
    mixer_input,
    mixer_gain,
    query_one,
    query_two,
    key_one,
    key_two,
    value_weight,
    lambdas,
    head_gain,
    output_weight,
    expert_input,
    expert_gain,
    routes,
    route_weight,
    expert_gate,
    expert_up,
    expert_down,
    shared_gate,
    shared_up,
    shared_down,
):
    ep_size = lax.axis_size("ep")
    tp_size = lax.axis_size("tp")
    ep_rank = lax.axis_index("ep")
    mixer_rows = mixer_input.shape[0]
    half_rows = mixer_rows // 2
    model_width = mixer_input.shape[1]
    query_cols = query_one.shape[1]
    key_cols = key_one.shape[1]
    value_dim = head_gain.shape[0]
    local_kv = key_cols // HEAD
    local_heads = query_cols // HEAD
    group_size = local_heads // local_kv
    top_bit = ep_size.bit_length() - 2
    normed = normalize(mixer_input, mixer_gain)
    joined_weight = jnp.concatenate([query_one, query_two, key_one, key_two, value_weight], axis=1)
    projected = jnp.dot(normed, joined_weight, preferred_element_type=jnp.float32).astype(
        jnp.bfloat16
    )
    query_part = projected[:, : 2 * query_cols]
    key_values = projected[:, 2 * query_cols :]
    low_start = ep_rank * mixer_rows
    high_queries = query_part[half_rows:]
    high_queries = partner_2(high_queries, "ep", top_bit)
    partner = jnp.where(ep_rank >= ep_size // 2, ep_rank - ep_size // 2, ep_rank + ep_size // 2)
    high_start = partner * mixer_rows + half_rows

    def split_queries(query_rows):
        query_first = (
            query_rows[:, :query_cols]
            .reshape(half_rows, local_kv, group_size, HEAD)
            .transpose(1, 2, 0, 3)
        )
        query_second = (
            query_rows[:, query_cols:]
            .reshape(half_rows, local_kv, group_size, HEAD)
            .transpose(1, 2, 0, 3)
        )
        return (query_first, query_second)

    def heads_of(key_rows):
        return key_rows.reshape(half_rows, local_kv, HEAD).transpose(1, 0, 2)

    query_sets = (split_queries(query_part[:half_rows]), split_queries(high_queries))
    query_starts = (low_start, high_start)
    stat_shape = (2, 2, local_kv, group_size, half_rows)
    initial = (
        jnp.full(stat_shape, NEG, jnp.float32),
        jnp.zeros(stat_shape, jnp.float32),
        jnp.zeros(stat_shape + (value_dim,), jnp.float32),
    )
    arrived = lax.all_gather(key_values, "ep", axis=0, tiled=True)
    shard_count = arrived.shape[0] // mixer_rows

    def one_shard(shard_index, current):
        for key_half in range(2):
            key_block = lax.dynamic_slice_in_dim(
                arrived, shard_index * mixer_rows + key_half * half_rows, half_rows, 0
            )
            key_pair = (
                heads_of(key_block[:, :key_cols]),
                heads_of(key_block[:, key_cols : 2 * key_cols]),
            )
            value_rows = (
                key_block[:, 2 * key_cols :]
                .reshape(half_rows, local_kv, value_dim)
                .transpose(1, 0, 2)
            )
            key_start = shard_index * mixer_rows + key_half * half_rows
            for which_half in range(2):

                def update(
                    state_in,
                    chosen=which_half,
                    key_pair=key_pair,
                    value_rows=value_rows,
                    key_begin=key_start,
                ):
                    return attend(
                        state_in,
                        chosen,
                        query_sets[chosen],
                        key_pair,
                        value_rows,
                        query_starts[chosen],
                        key_begin,
                    )

                current = lax.cond(
                    key_start <= query_starts[which_half], update, unchanged, current
                )
        return current

    maxima, totals, weighted = lax.fori_loop(0, shard_count, one_shard, initial)
    mixed = weighted / totals[..., None]
    lambda_grid = lambdas.reshape(local_kv, group_size)[None, :, :, None, None]
    combined = mixed[:, 0] - lambda_grid * mixed[:, 1]
    factor = lax.rsqrt(jnp.mean(combined * combined, axis=-1, keepdims=True) + EPS)
    normed_heads = (combined * factor * head_gain).astype(jnp.bfloat16)
    head_halves = normed_heads.transpose(0, 3, 1, 2, 4).reshape(
        2, half_rows, local_heads * value_dim
    )
    high_rows = head_halves[1]
    high_rows = partner_2(high_rows, "ep", top_bit)
    head_rows = jnp.concatenate([head_halves[0], high_rows], axis=0)
    token_rows = expert_input.shape[0]
    normed_experts = normalize(expert_input, expert_gain)
    experts_local = expert_gate.shape[0]
    expert_count = experts_local * ep_size
    top_count = routes.shape[1]
    capacity = max(2, 5 * token_rows * top_count // (4 * expert_count))
    slot_count = expert_count * capacity
    flat_routes = routes.reshape(-1)
    onehot = (flat_routes[:, None] == jnp.arange(expert_count, dtype=jnp.int32)[None, :]).astype(
        jnp.int32
    )
    slot_place = jnp.sum((jnp.cumsum(onehot, axis=0) - onehot) * onehot, axis=1)
    slot_ids = (flat_routes * capacity + slot_place).reshape(token_rows, top_count)
    slot_match = jnp.arange(slot_count, dtype=jnp.int32)[:, None, None] == slot_ids[None, :, :]
    select = jnp.any(slot_match, axis=2).astype(jnp.bfloat16)
    outgoing = jnp.dot(select, normed_experts, preferred_element_type=jnp.float32).astype(
        jnp.bfloat16
    )
    outgoing = outgoing.reshape(ep_size, experts_local * capacity, model_width)
    received = lax.all_to_all(outgoing, "ep", split_axis=0, concat_axis=0, tiled=True)
    expert_rows, slot_rows = one_gather((normed_experts, received), "tp", (0, 0))
    slot_grid = slot_rows.reshape(tp_size, ep_size, experts_local, capacity, model_width)
    gated = jnp.einsum(
        "tsecd,edf->tsecf", slot_grid, expert_gate, preferred_element_type=jnp.float32
    )
    lifted = jnp.einsum(
        "tsecd,edf->tsecf", slot_grid, expert_up, preferred_element_type=jnp.float32
    )
    routed_hidden = (jax.nn.silu(gated) * lifted).astype(jnp.bfloat16)
    shared_gated = jnp.dot(expert_rows, shared_gate, preferred_element_type=jnp.float32)
    shared_lifted = jnp.dot(expert_rows, shared_up, preferred_element_type=jnp.float32)
    shared_hidden = (jax.nn.silu(shared_gated) * shared_lifted).astype(jnp.bfloat16)
    routed_slots = ep_size * experts_local * capacity
    expert_block = token_rows + routed_slots
    mixer_sum = sum_at_owner(
        jnp.dot(head_rows, output_weight, preferred_element_type=jnp.float32).astype(jnp.bfloat16),
        "tp",
        0,
    )
    block_count = expert_block * lax.axis_size("tp") // expert_block
    shared_part = jnp.dot(shared_hidden, shared_down, preferred_element_type=jnp.float32).reshape(
        block_count, token_rows, model_width
    )
    routed_part = jnp.einsum(
        "tsecf,efd->tsecd", routed_hidden, expert_down, preferred_element_type=jnp.float32
    ).reshape(block_count, routed_slots, model_width)
    expert_sum = sum_at_owner(
        jnp.concatenate([shared_part, routed_part], axis=1)
        .reshape(expert_block * lax.axis_size("tp"), model_width)
        .astype(jnp.bfloat16),
        "tp",
        0,
    )
    mixer_output = mixer_sum.astype(jnp.bfloat16)
    shared_result = expert_sum[:token_rows]
    routed_result = (
        expert_sum[token_rows:]
        .astype(jnp.bfloat16)
        .reshape(ep_size, experts_local * capacity, model_width)
    )
    returned = lax.all_to_all(routed_result, "ep", split_axis=0, concat_axis=0, tiled=True).reshape(
        slot_count, model_width
    )
    picked = returned[slot_ids].astype(jnp.float32)
    routed_total = jnp.sum(picked * route_weight[:, :, None], axis=1)
    expert_output = (routed_total + shared_result).astype(jnp.bfloat16)
    return (mixer_output, expert_output)


def solution(mesh):
    in_specs = (
        P("ep", None),
        P(),
        P(None, "tp"),
        P(None, "tp"),
        P(None, "tp"),
        P(None, "tp"),
        P(None, "tp"),
        P("tp"),
        P(),
        P("tp", None),
        P(("ep", "tp"), None),
        P(),
        P(("ep", "tp"), None),
        P(("ep", "tp"), None),
        P("ep", None, "tp"),
        P("ep", None, "tp"),
        P("ep", "tp", None),
        P(None, "tp"),
        P(None, "tp"),
        P("tp", None),
    )
    out_specs = (P(("ep", "tp"), None), P(("ep", "tp"), None))
    return jax.shard_map(body, mesh=mesh, in_specs=in_specs, out_specs=out_specs, check_vma=False)
```

profile of v0, /device:TPU:1, one launch (start us, length us, event | category | flops | bytes accessed | tf_op | source)
XLA Modules:
  0.0 1259.1 jit_solution(7981876406648956897)
XLA Ops:
  11.5 1.6 convolution_convert_fusion.1
  13.1 1.6 reshape.1965
  14.8 13.1 %all-to-all-start.1 = ((bf16[64,5,2048]{2,1,0:T(8,128)(2,1)}), bf16[64,5,2048]{2,1,0:T(8,128)(2,1)S(1)}, u32[]{:S(2)}, u32[]{:S(2)}) async-start(bf16[64,5,2048]{2,1,0:T(8,128)(2,1)} %reshape.1965), calls=%async_computation.1 | async-start | bytes 4194304 | tf_op jit(solution)/shard_map/all_to_all | solution.py:240
  30.1 47.5 %all-to-all-done.1 = bf16[64,5,2048]{2,1,0:T(8,128)(2,1)S(1)} async-done(((bf16[64,5,2048]{2,1,0:T(8,128)(2,1)}), bf16[64,5,2048]{2,1,0:T(8,128)(2,1)S(1)}, u32[]{:S(2)}, u32[]{:S(2)}) %all-to-all-start.1) | async-done | bytes 1310752 | tf_op jit(solution)/shard_map/all_to_all | solution.py:240
  77.6 2.6 reshape.1966
  80.2 2.8 pad_maximum_fusion.1
  84.2 5.0 concatenate.69
  89.5 2.3 convolution_convert_fusion.3
  92.6 2.9 collective-permute-start
  95.7 4.0 collective-permute-done
  99.9 57.8 %all-gather.6.cloned.1.call-done = bf16[3670016]{0:T(1024)(128)(2,1)} async-done(((bf16[917504]{0:T(1024)(128)(2,1)}), bf16[3670016]{0:T(1024)(128)(2,1)}) %all-gather.6.cloned.1.call-update) | async-done | bytes 7340048 | tf_op jit(solution)/shard_map/all_gather | solution.py:31
  157.7 8.8 reshape.1984
  166.5 7.6 slice.1063
  174.1 3.3 reshape_reshape.3
  177.4 2.5 fusion.187
  179.9 4.9 convolution_convert_fusion
  184.8 3.2 copy.167
  188.0 9.8 reshape.1968
  197.8 10.2 fusion.127
  208.0 6.9 fusion.139
  215.0 1.7 convert_bitcast_fusion
  216.7 6.3 copy.166
  223.0 10.3 pad_maximum_fusion
  233.3 10.4 copy.168
  243.7 5.5 all-to-all-start.2
  249.2 12.0 copy.156
  261.2 210.8 %while.43 = (s32[]{:T(128)}, f32[2,2,1,2,128]{4,3,2,1,0:T(2,128)S(1)}, f32[2,2,1,2,128]{4,3,2,1,0:T(2,128)S(1)}, f32[2,2,1,2,128,128]{5,4,3,2,1,0:T(8,128)S(1)},...) while((s32[]{:T(128)}, ...), condition=%wide.region_26.27_spmd, body=%wide.region_1.26_spmd.sunk | while | flops 103623184 | bytes 8866761 | solution.py:209
  262.8 5.4 conditional.8
  266.9 1.4 fusion.1
  269.6 5.7 conditional.10
  273.8 1.5 fusion.61
  275.3 1.3 conditional.11
  278.3 5.4 conditional.8
  282.3 1.4 fusion.1
  285.0 1.3 conditional.11
  297.8 1.3 conditional.11
  306.3 1.3 conditional.11
  310.5 1.3 conditional.11
  319.0 1.3 conditional.11
  327.6 1.3 conditional.11
  336.1 1.3 conditional.11
  340.3 1.3 conditional.11
  344.6 1.3 conditional.11
  353.1 1.3 conditional.11
  361.6 1.3 conditional.11
  370.1 1.3 conditional.11
  382.8 1.3 conditional.11
  391.3 1.3 conditional.11
  404.0 1.3 conditional.11
  421.0 1.3 conditional.11
  473.0 281.0 %collective-permute-start.1 = (bf16[128,256]{0,1:T(8,128)(2,1)S(1)}, bf16[128,256]{0,1:T(8,128)(2,1)S(1)}, u32[]{:S(2)}, u32[]{:S(2)}) collective-permute-start(bf16[128,256]{0,1:T(8,128)(2,1)S(1)} %bitcast.453), channel_id=1, source_target_pairs={{0,128},{128,0},{4,132},{132,4},{8,136},{136,8},{12,140},{140,12},... | collective-permute-start | bytes 196616 | tf_op jit(solution)/shard_map/ppermute | solution.py:20
  754.0 1.7 collective-permute-done.1
  755.6 1.5 convolution_convert_fusion.2
  757.1 4.2 all-to-all-start
  761.3 5.2 convert_reduce_fusion
  766.4 1.8 copy-done.3
  768.4 1.6 reshape.1974
  771.0 420.7 %all-to-all-start.3 = ((bf16[64,5,2048]{2,1,0:T(8,128)(2,1)}), bf16[64,5,2048]{2,1,0:T(8,128)(2,1)}, u32[]{:S(2)}, u32[]{:S(2)}) async-start(bf16[64,5,2048]{2,1,0:T(8,128)(2,1)} %reshape.1974), calls=%async_computation.3 | async-start | bytes 4194304 | tf_op jit(solution)/shard_map/all_to_all | solution.py:281
  1193.0 48.1 %all-to-all-done.3 = bf16[64,5,2048]{2,1,0:T(8,128)(2,1)} async-done(((bf16[64,5,2048]{2,1,0:T(8,128)(2,1)}), bf16[64,5,2048]{2,1,0:T(8,128)(2,1)}, u32[]{:S(2)}, u32[]{:S(2)}) %all-to-all-start.3) | async-done | bytes 1310752 | tf_op jit(solution)/shard_map/all_to_all | solution.py:281
  1241.1 2.6 reshape.1975
  1243.7 1.4 gather_fusion
  1245.1 1.3 reshape.1987
  1246.4 3.2 multiply_reduce_fusion
  1249.6 2.2 fusion.147
  (1591 shorter events, 275.8 us)
Async XLA Ops:
  7.2 207.8 %copy-start = (bf16[1,256,2048]{2,1,0:T(8,128)(2,1)S(1)}, bf16[1,256,2048]{2,1,0:T(8,128)(2,1)}, u32[]{:S(2)}) copy-start(bf16[1,256,2048]{2,1,0:T(8,128)(2,1)} %param.94) | copy-start | bytes 3145732
  14.8 13.2 %copy-start.9 = (f32[2048]{0:T(1024)S(1)}, f32[2048]{0:T(1024)}, u32[]{:S(2)}) copy-start(f32[2048]{0:T(1024)} %param.89) | copy-start | bytes 24580
  14.8 62.8 %all-to-all-start.1 = ((bf16[64,5,2048]{2,1,0:T(8,128)(2,1)}), bf16[64,5,2048]{2,1,0:T(8,128)(2,1)S(1)}, u32[]{:S(2)}, u32[]{:S(2)}) async-start(bf16[64,5,2048]{2,1,0:T(8,128)(2,1)} %reshape.1965), calls=%async_computation.1 | async-start | bytes 4194304 | tf_op jit(solution)/shard_map/all_to_all | solution.py:240
  27.9 129.8 %all-gather.6.cloned.1.call-start = ((), (), s32[]{:S(2)}) async-start(), calls=%async_computation.5 | async-start | bytes 9175040 | tf_op jit(solution)/shard_map/all_gather | solution.py:31
  80.2 2.9 copy-start.7
  83.0 0.9 copy-start.8
  83.0 166.2 %all-gather.4.cloned.1.call-start = ((), (), s32[]{:S(2)}) async-start(), calls=%async_computation.4 | async-start | bytes 8519680 | tf_op jit(solution)/shard_map/all_gather | solution.py:167
  84.2 5.0 copy-start.5
  84.2 5.3 copy-start.14
  92.6 7.1 collective-permute-start
  166.5 7.6 slice-start
  177.3 2.5 copy-start.2
  197.8 10.2 copy-start.4
  197.8 10.2 copy-start.13
  243.7 513.4 %all-to-all-start.2 = ((bf16[4,448,2048]{2,1,0:T(8,128)(2,1)}), bf16[4,448,2048]{2,1,0:T(8,128)(2,1)}, u32[]{:S(2)}, u32[]{:S(2)}) async-start(bf16[4,448,2048]{2,1,0:T(8,128)(2,1)} %copy.168), calls=%async_computation.2 | async-start | bytes 14680064 | tf_op jit(solution)/shard_map/all_to_all | solution.py:47
  472.1 0.7 copy-start.10
  472.1 0.8 copy-start.12
  472.1 283.5 %copy-start.6 = (bf16[256,2048]{1,0:T(8,128)(2,1)S(1)}, bf16[256,2048]{1,0:T(8,128)(2,1)}, u32[]{:S(2)}) copy-start(bf16[256,2048]{1,0:T(8,128)(2,1)} %param.87) | copy-start | bytes 3145732
  473.0 282.6 %collective-permute-start.1 = (bf16[128,256]{0,1:T(8,128)(2,1)S(1)}, bf16[128,256]{0,1:T(8,128)(2,1)S(1)}, u32[]{:S(2)}, u32[]{:S(2)}) collective-permute-start(bf16[128,256]{0,1:T(8,128)(2,1)S(1)} %bitcast.453), channel_id=1, source_target_pairs={{0,128},{128,0},{4,132},{132,4},{8,136},{136,8},{12,140},{140,12},... | collective-permute-start | bytes 196616 | tf_op jit(solution)/shard_map/ppermute | solution.py:20
  757.1 13.9 %all-to-all-start = ((bf16[4,64,2048]{2,1,0:T(8,128)(2,1)}), bf16[4,64,2048]{2,1,0:T(8,128)(2,1)S(1)}, u32[]{:S(2)}, u32[]{:S(2)}) async-start(bf16[4,64,2048]{2,1,0:T(8,128)(2,1)} %bitcast.97), calls=%async_computation | async-start | bytes 2097152 | tf_op jit(solution)/shard_map/all_to_all | solution.py:47
  766.4 1.8 copy-start.3
  770.0 422.0 %copy-start.11 = (f32[128,2]{0,1:T(2,128)S(1)}, f32[128,2]{0,1:T(2,128)}, u32[]{:S(2)}) copy-start(f32[128,2]{0,1:T(2,128)} %param.91) | copy-start | bytes 3076
  771.0 470.1 %all-to-all-start.3 = ((bf16[64,5,2048]{2,1,0:T(8,128)(2,1)}), bf16[64,5,2048]{2,1,0:T(8,128)(2,1)}, u32[]{:S(2)}, u32[]{:S(2)}) async-start(bf16[64,5,2048]{2,1,0:T(8,128)(2,1)} %reshape.1974), calls=%async_computation.3 | async-start | bytes 4194304 | tf_op jit(solution)/shard_map/all_to_all | solution.py:281
  1246.4 5.4 copy-start.1
Sparse Core Ops, SparseCore 0:
  83.1 74.5 all-gather.5
  161.0 84.3 all-gather.3
where the time goes:
time: 1280 us; the launch traced here: 1260 us
  starting transfers between devices  727 us (57%)
  local copies, waits for them, and re-layouts  192 us (15%)
  waiting for transfers between devices  160 us (12%)
  matrix products  98.2 us (8%)
  other arithmetic  55.7 us (4%)
  between operations  14.9 us (1%)
    all_to_all x1, starting transfers between devices, body(): lax.all_to_all(routed_result, 'ep', split_axis=0, concat_axis=0, tiled=True)  421 us
    ppermute x2, starting transfers between devices, partner_2(): return lax.ppermute(block, axis, route)  284 us
    all_gather x1, waiting for transfers between devices, one_gather(): lines, at, done = (lax.all_gather(flat, axis), 0, [])  57.8 us
    reshape x64, local copies, waits for them, and re-layouts, heads_of(): return key_rows.reshape(half_rows, local_kv, HEAD).transpose(1, 0, 2)  50.3 us
    reshape x64, local copies, waits for them, and re-layouts, one_shard(): value_rows = key_block[:, 2 * key_cols:].reshape(half_rows, local_kv, val...  49.9 us
    all_to_all x1, waiting for transfers between devices, body(): lax.all_to_all(routed_result, 'ep', split_axis=0, concat_axis=0, tiled=True)  48.1 us
    all_to_all x1, waiting for transfers between devices, body(): lax.all_to_all(outgoing, 'ep', split_axis=0, concat_axis=0, tiled=True)  47.5 us
    dot_general x142, matrix products, attend(): jnp.einsum('kgqj,kjd->kgqd', weights.astype(jnp.bfloat16), value_rows, pr...  33.8 us
  transfers between devices with their start and end apart: 8, of which 6 were waited for; matrix products, arithmetic and copies ran while one was open for 25% of the time, Pallas kernels for 0%

commit v1 on v0

v1 whole, which is shorter than its diff:
```python
import functools

import jax
import jax.numpy as jnp
from jax import lax
from jax.experimental import pallas as pl
from jax.experimental.pallas import tpu as pltpu
from jax.sharding import PartitionSpec as P

HEAD = 64

EPS = 1e-06
NEG = -1e30
MESH = pl.DeviceIdType.MESH

SPAN = 2


def normalize(activations, scaling):
    values = activations.astype(jnp.float32)
    factor = lax.rsqrt(jnp.mean(values * values, axis=-1, keepdims=True) + EPS)
    return (values * factor * scaling).astype(jnp.bfloat16)


def swap_high(block, axis):
    count = lax.axis_size(axis)
    return lax.ppermute(block, axis, [(i, count - 1 - i) for i in range(count)])


def attention_kernel(rank_ref, low_ref, high_ref, kv_ref, lam_ref, gain_ref, out_ref, query, maxima, totals, weighted):
    shards, block_rows, _ = kv_ref.shape
    rows = block_rows // 2
    half = rows // 2
    span_keys = SPAN * rows
    rank = rank_ref[0]
    zeros = jnp.zeros((HEAD, 2 * half), jnp.bfloat16)
    for which, source in enumerate((low_ref, high_ref)):
        first = jnp.concatenate([source[0:HEAD], source[HEAD : 2 * HEAD]], axis=1)
        second = jnp.concatenate([source[2 * HEAD : 3 * HEAD], source[3 * HEAD : 4 * HEAD]], axis=1)
        query[which, 0, 0:HEAD] = first
        query[which, 0, HEAD : 2 * HEAD] = zeros
        query[which, 1, 0:HEAD] = zeros
        query[which, 1, HEAD : 2 * HEAD] = second

    def block(which, shard, masked, query_start):
        keys = kv_ref[pl.ds(shard, SPAN), 0:rows, :].reshape(span_keys, 2 * HEAD)
        values = [kv_ref[shard + i, rows + j * half : rows + (j + 1) * half, :] for i in range(SPAN) for j in range(2)]
        values = jnp.concatenate(values, axis=1)
        if masked:
            key_pos = shard * rows + lax.broadcasted_iota(jnp.int32, (span_keys, 2 * half), 0)
            lane = lax.broadcasted_iota(jnp.int32, (span_keys, 2 * half), 1)
            query_pos = query_start + jnp.where(lane >= half, lane - half, lane)
            visible = key_pos <= query_pos
        for m in range(2):
            scores = jnp.dot(keys, query[which, m], preferred_element_type=jnp.float32)
            if masked:
                scores = jnp.where(visible, scores, NEG)
            earlier = maxima[which, m]
            latest = jnp.maximum(earlier, jnp.max(scores, axis=0, keepdims=True))
            shrink = jnp.exp(earlier - latest)
            weights = jnp.exp(scores - latest)
            if masked:
                weights = jnp.where(visible, weights, 0.0)
            totals[which, m] = totals[which, m] * shrink + jnp.sum(weights, axis=0, keepdims=True)
            product = jnp.dot(values, weights.astype(jnp.bfloat16), preferred_element_type=jnp.float32)
            weighted[which, m] = weighted[which, m] * shrink + product
            maxima[which, m] = latest

    for which in range(2):
        maxima[which] = jnp.full(maxima.shape[1:], NEG, jnp.float32)
        totals[which] = jnp.zeros(totals.shape[1:], jnp.float32)
        weighted[which] = jnp.zeros(weighted.shape[1:], jnp.float32)
        full = rank if which == 0 else shards - 1 - rank
        steps = full // SPAN

        def step(i, carry, which=which):
            block(which, i * SPAN, False, 0)
            return carry

        lax.fori_loop(0, steps, step, 0)
        block(which, steps * SPAN, True, full * rows + which * half)
        mixed = [weighted[which, m] / totals[which, m] for m in range(2)]
        combined = mixed[0] - lam_ref[...] * mixed[1]
        factor = lax.rsqrt(jnp.mean(combined * combined, axis=0, keepdims=True) + EPS)
        normed = combined * factor * gain_ref[...]
        for head in range(2):
            part = normed[:, head * half : (head + 1) * half]
            out_ref[which, :, head * 128 : (head + 1) * 128] = part.T.astype(jnp.bfloat16)


def attend(rank, low, high, kv, lambdas, head_gain):
    shards, block_rows, _ = kv.shape
    half = block_rows // 4
    value_dim = head_gain.shape[0]
    pairs = shards * half * 2
    lam = jnp.repeat(lambdas, half).reshape(1, 2 * half)
    vmem = pl.BlockSpec(memory_space=pltpu.VMEM)
    return pl.pallas_call(
        attention_kernel,
        out_shape=jax.ShapeDtypeStruct((2, half, 2 * value_dim), jnp.bfloat16),
        in_specs=[pl.BlockSpec(memory_space=pltpu.SMEM)] + [vmem] * 5,
        out_specs=vmem,
        scratch_shapes=[
            pltpu.VMEM((2, 2, 2 * HEAD, 2 * half), jnp.bfloat16),
            pltpu.VMEM((2, 2, 1, 2 * half), jnp.float32),
            pltpu.VMEM((2, 2, 1, 2 * half), jnp.float32),
            pltpu.VMEM((2, 2, value_dim, 2 * half), jnp.float32),
        ],
        cost_estimate=pl.CostEstimate(flops=pairs * 2 * half * 2 * 512, bytes_accessed=kv.size * 2, transcendentals=pairs * 2 * half * 2),
        compiler_params=pltpu.CompilerParams(vmem_limit_bytes=40 * 1024 * 1024),
        name="attend",
    )(rank.reshape(1), low, high, kv, lam, head_gain.reshape(value_dim, 1))


def expert_kernel(rows_ref, gate_ref, up_ref, down_ref, out_ref, total):
    group = pl.program_id(0)
    rows = rows_ref[...]
    gated = jnp.dot(rows, gate_ref[0], preferred_element_type=jnp.float32)
    lifted = jnp.dot(rows, up_ref[0], preferred_element_type=jnp.float32)
    hidden = (gated / (1.0 + jnp.exp(-gated)) * lifted).astype(jnp.bfloat16)
    part = jnp.dot(hidden, down_ref[0], preferred_element_type=jnp.float32)
    part = part.astype(jnp.bfloat16).astype(jnp.float32)

    @pl.when(group == 0)
    def _():
        total[...] = part

    @pl.when(group > 0)
    def _():
        total[...] += part

    @pl.when(group == pl.num_programs(0) - 1)
    def _():
        out_ref[...] = total[...].astype(out_ref.dtype)


def swiglu_groups(rows, gate, up, down, kind, name):
    groups, width, hidden = gate.shape
    count = rows.shape[0]
    return pl.pallas_call(
        expert_kernel,
        out_shape=jax.ShapeDtypeStruct((count, width), kind),
        grid=(groups,),
        in_specs=[
            pl.BlockSpec((count, width), lambda g: (0, 0)),
            pl.BlockSpec((1, width, hidden), lambda g: (g, 0, 0)),
            pl.BlockSpec((1, width, hidden), lambda g: (g, 0, 0)),
            pl.BlockSpec((1, hidden, width), lambda g: (g, 0, 0)),
        ],
        out_specs=pl.BlockSpec((count, width), lambda g: (0, 0)),
        scratch_shapes=[pltpu.VMEM((count, width), jnp.float32)],
        cost_estimate=pl.CostEstimate(flops=groups * count * width * hidden * 6, bytes_accessed=groups * width * hidden * 6, transcendentals=groups * count * hidden),
        compiler_params=pltpu.CompilerParams(vmem_limit_bytes=60 * 1024 * 1024),
        name=name,
    )(rows, gate, up, down)


def weight_kernel(*refs):
    count = (len(refs) - 7) // 2
    sources, targets = refs[:count], refs[count : 2 * count]
    send_own, recv_own, send_on, recv_on, send_pair, recv_pair, local = refs[2 * count :]
    size = lax.axis_size("tp")
    me = lax.axis_index("tp")
    place = lax.axis_index("ep")
    core = lax.rem(place, 2)
    right, left = {"tp": lax.rem(me + 1, size)}, {"tp": lax.rem(me + size - 1, size)}
    other = {"ep": place + 1 - 2 * core}
    sides = (right, left)
    first_shared = count - 3

    barrier = pltpu.get_barrier_semaphore()
    for peer in (right, left, other):
        pl.semaphore_signal(barrier, inc=1, device_id=peer, device_id_type=MESH)
    pl.semaphore_wait(barrier, 3)

    def span_of(i):
        rows = sources[i].shape[0]
        return (rows, 0) if i < first_shared else (rows // 2, core * (rows // 2))

    def piece(ref, i, part):
        rows, start = span_of(i)
        return ref.at[pl.ds(start + part * (rows // 2), rows // 2)]

    def whole(ref, i):
        rows, start = span_of(i)
        return ref.at[pl.ds(start, rows)]

    def send(source, target, send_sem, recv_sem, peer):
        copy = pltpu.make_async_remote_copy(
            src_ref=source, dst_ref=target, send_sem=send_sem, recv_sem=recv_sem, device_id=peer, device_id_type=MESH
        )
        copy.start()
        return copy

    items = tuple(range(first_shared, count)) + tuple(range(first_shared))
    own, onward, pairs = {}, {}, []
    for order in range(2):
        for i in items:
            for side in range(2):
                part = side if order == 0 else 1 - side
                own[side, order, i] = send(
                    piece(sources[i], i, part),
                    piece(targets[i].at[me], i, part),
                    send_own.at[side, order, i],
                    recv_own.at[side, order, i],
                    sides[side],
                )
    kept = []
    for i in items:
        copy = pltpu.make_async_copy(sources[i], targets[i].at[me], local.at[i])
        copy.start()
        kept.append(copy)

    for i in items:
        for side in range(2):
            own[side, 0, i].wait_recv()
            view = piece(targets[i].at[sides[1 - side]["tp"]], i, side)
            onward[side, i] = send(view, view, send_on.at[side, i], recv_on.at[side, i], sides[side])

    def to_other(owner, i, k):
        view = whole(targets[i].at[owner], i)
        pairs.append(send(view, view, send_pair.at[k, i - first_shared], recv_pair.at[k, i - first_shared], other))

    for i in items[:3]:
        for side in range(2):
            own[side, 1, i].wait_recv()
            to_other(sides[1 - side]["tp"], i, side)
    for i in items[:3]:
        for side in range(2):
            onward[side, i].wait_recv()
        to_other(lax.rem(me + 2, size), i, 2)
    for i in items[3:]:
        for side in range(2):
            own[side, 1, i].wait_recv()
            onward[side, i].wait_recv()
    for copy in kept:
        copy.wait()
    for copy in pairs:
        copy.wait_recv()
        copy.wait_send()
    for i in items:
        for side in range(2):
            own[side, 0, i].wait_send()
            own[side, 1, i].wait_send()
            onward[side, i].wait_send()


def gather_weights(*weights):
    size = lax.axis_size("tp")
    hbm = pl.BlockSpec(memory_space=pltpu.HBM)
    dma = pltpu.SemaphoreType.DMA
    count = len(weights)
    return pl.pallas_call(
        weight_kernel,
        out_shape=[jax.ShapeDtypeStruct((size,) + w.shape, w.dtype) for w in weights],
        in_specs=[hbm] * count,
        out_specs=[hbm] * count,
        scratch_shapes=[dma((2, 2, count))] * 2 + [dma((2, count))] * 2 + [dma((3, 3))] * 2 + [dma((count,))],
        cost_estimate=pl.CostEstimate(flops=0, bytes_accessed=300_000_000, transcendentals=0),
        compiler_params=pltpu.CompilerParams(collective_id=0, has_side_effects=True, vmem_limit_bytes=60 * 1024 * 1024),
        name="gather_weights",
    )(*weights)


def body(
    mixer_input,
    mixer_gain,
    query_one,
    query_two,
    key_one,
    key_two,
    value_weight,
    lambdas,
    head_gain,
    output_weight,
    expert_input,
    expert_gain,
    routes,
    route_weight,
    expert_gate,
    expert_up,
    expert_down,
    shared_gate,
    shared_up,
    shared_down,
):
    ep_size = lax.axis_size("ep")
    tp_size = lax.axis_size("tp")
    ep_rank = lax.axis_index("ep")
    mixer_rows, model_width = mixer_input.shape
    half_rows = mixer_rows // 2
    token_rows = expert_input.shape[0]

    gate_all = lax.all_gather(expert_gate[0], "tp")

    normed = normalize(mixer_input, mixer_gain)
    query_cols = query_one.shape[1]
    turned_weight = jnp.concatenate([query_one, query_two, value_weight], axis=1)
    turned = lax.dot_general(turned_weight, normed, (((0,), (1,)), ((), ())), preferred_element_type=jnp.float32)
    keys = jnp.dot(normed, jnp.concatenate([key_one, key_two], axis=1), preferred_element_type=jnp.float32)
    keys = keys.astype(jnp.bfloat16)
    queries = (turned[: 2 * query_cols].astype(jnp.bfloat16) * HEAD ** (-0.5)).astype(jnp.bfloat16)
    values = turned[2 * query_cols :].astype(jnp.bfloat16)
    key_values = jnp.concatenate([keys, values[:, :half_rows], values[:, half_rows:]], axis=0)
    arrived = lax.all_gather(key_values, "ep")
    high_queries = swap_high(queries[:, half_rows:], "ep")

    normed_experts = normalize(expert_input, expert_gain)
    expert_count = expert_gate.shape[0] * ep_size
    top_count = routes.shape[1]
    capacity = max(2, 5 * token_rows * top_count // (4 * expert_count))
    slot_count = expert_count * capacity
    flat_routes = routes.reshape(-1)
    onehot = (flat_routes[:, None] == jnp.arange(expert_count, dtype=jnp.int32)[None, :]).astype(jnp.bfloat16)
    before = jnp.tril(jnp.ones((token_rows * top_count, token_rows * top_count), jnp.bfloat16), -1)
    counts = jnp.dot(before, onehot, preferred_element_type=jnp.float32)
    slot_place = jnp.sum(counts * onehot, axis=1).astype(jnp.int32)
    slot_ids = (flat_routes * capacity + slot_place).reshape(token_rows, top_count)
    slot_match = jnp.arange(slot_count, dtype=jnp.int32)[:, None, None] == slot_ids[None, :, :]
    select = jnp.any(slot_match, axis=2).astype(jnp.bfloat16)
    outgoing = jnp.dot(select, normed_experts, preferred_element_type=jnp.float32).astype(jnp.bfloat16)
    lines = slot_count // ep_size * model_width // 128
    outgoing = outgoing.reshape(ep_size, lines, 128)
    outgoing, high_queries = lax.optimization_barrier((outgoing, high_queries))
    received = lax.all_to_all(outgoing, "ep", split_axis=0, concat_axis=0, tiled=True)

    up_all, down_all, shared_gate_all, shared_up_all, shared_down_all = gather_weights(
        expert_up[0], expert_down[0], shared_gate, shared_up, shared_down
    )

    halves = attend(ep_rank, queries[:, :half_rows], high_queries, arrived, lambdas, head_gain)
    slot_rows = received.reshape(slot_count, model_width)
    routed_result = swiglu_groups(slot_rows, gate_all, up_all, down_all, jnp.bfloat16, "routed")
    shared_result = swiglu_groups(
        normed_experts, shared_gate_all, shared_up_all, shared_down_all, jnp.float32, "shared"
    )
    routed_result = routed_result.reshape(ep_size, lines, 128)
    returned = lax.all_to_all(routed_result, "ep", split_axis=0, concat_axis=0, tiled=True)
    returned, halves, shared_result = lax.optimization_barrier((returned, halves, shared_result))
    returned = returned.reshape(slot_count, model_width)
    picks = slot_ids[:, :, None] == jnp.arange(slot_count, dtype=jnp.int32)[None, None, :]
    picks = picks.astype(jnp.bfloat16)
    routed_total = jnp.zeros((token_rows, model_width), jnp.float32)
    for k in range(top_count):
        picked = jnp.dot(picks[:, k], returned, preferred_element_type=jnp.float32)
        routed_total = routed_total + picked * route_weight[:, k : k + 1]
    high_rows = swap_high(halves[1], "ep")
    head_rows = jnp.concatenate([halves[0], high_rows], axis=0)
    partial = jnp.dot(head_rows, output_weight, preferred_element_type=jnp.float32).astype(jnp.bfloat16)
    partial = partial.reshape(tp_size, mixer_rows // tp_size, model_width)
    tp_rank = lax.axis_index("tp")
    mixer_sum = lax.dynamic_index_in_dim(partial, tp_rank, 0, keepdims=False).astype(jnp.float32)
    for step in range(1, tp_size):
        leaving = lax.dynamic_index_in_dim(partial, lax.rem(tp_rank + step, tp_size), 0, keepdims=False)
        part = lax.ppermute(leaving, "tp", [(i, (i + step) % tp_size) for i in range(tp_size)])
        mixer_sum = mixer_sum + part.astype(jnp.float32)
    mixer_output = mixer_sum.astype(jnp.bfloat16)
    expert_output = (routed_total + shared_result).astype(jnp.bfloat16)
    return (mixer_output, expert_output)


def solution(mesh):
    in_specs = (
        P("ep", None),
        P(),
        P(None, "tp"),
        P(None, "tp"),
        P(None, "tp"),
        P(None, "tp"),
        P(None, "tp"),
        P("tp"),
        P(),
        P("tp", None),
        P(("ep", "tp"), None),
        P(),
        P(("ep", "tp"), None),
        P(("ep", "tp"), None),
        P("ep", None, "tp"),
        P("ep", None, "tp"),
        P("ep", "tp", None),
        P(None, "tp"),
        P(None, "tp"),
        P("tp", None),
    )
    out_specs = (P(("ep", "tp"), None), P(("ep", "tp"), None))
    return jax.shard_map(body, mesh=mesh, in_specs=in_specs, out_specs=out_specs, check_vma=False)
```

time: 1280 us -> 258 us (0.20); the launches traced: 1260 us -> 257 us
  starting transfers between devices: 727 us -> 38.6 us
  local copies, waits for them, and re-layouts: 192 us -> 13.9 us
  Pallas kernels: 0 us -> 171 us
  waiting for transfers between devices: 160 us -> 10.5 us
  matrix products: 98.2 us -> 5.27 us
  other arithmetic: 55.7 us -> 3.55 us
    all_to_all x1, starting transfers between devices: 421 us -> 10.6 us  [body(): lax.all_to_all(routed_result, 'ep', split_axis=0, concat_axis=0, tiled=True)]
    ppermute x2 -> x5, starting transfers between devices: 284 us -> 18.5 us  [the longest x2 14.6 us: swap_high(): return lax.ppermute(block, axis, [(i, count - 1 - i) for i in range(count)])]
    pallas_call x0 -> x4, Pallas kernels: none -> 171 us  [the longest x1 123 us: gather_weights(): pl.pallas_call(weight_kernel, out_shape=[jax.ShapeDtypeStruct((size,) + w...]
    reshape x133 -> x5, local copies, waits for them, and re-layouts: 112 us -> 8.72 us  [the longest x1 3.29 us: body(): routed_result = routed_result.reshape(ep_size, lines, 128)]
    dot_general x290 -> x5, matrix products: 95.1 us -> 4.34 us  [the longest x1 1.79 us: body(): lax.dot_general(turned_weight, normed, (((0,), (1,)), ((), ())), preferre...]
    all_gather x2, waiting for transfers between devices: 57.8 us -> 0.02 us  [the longest x1 0.02 us: body(): arrived = lax.all_gather(key_values, 'ep')]
    all_to_all x1, waiting for transfers between devices: 48.1 us -> 0.01 us  [body(): lax.all_to_all(routed_result, 'ep', split_axis=0, concat_axis=0, tiled=True)]
    all_to_all x1, waiting for transfers between devices: 47.5 us -> 0.01 us  [body(): lax.all_to_all(outgoing, 'ep', split_axis=0, concat_axis=0, tiled=True)]
  transfers between devices with their start and end apart: 8 -> 9, of which waited for: 6 -> 3; matrix products, arithmetic and copies ran while one was open for 25% -> 7% of each run, Pallas kernels for 0% -> 66%
where the time goes in v1:
time: 258 us; the launch traced here: 257 us
  Pallas kernels  171 us (66%)
  starting transfers between devices  38.6 us (15%)
  between operations  14.5 us (6%)
  local copies, waits for them, and re-layouts  13.9 us (5%)
  waiting for transfers between devices  10.5 us (4%)
  matrix products  5.27 us (2%)
  other arithmetic  3.55 us (1%)
    pallas_call x1, Pallas kernels, gather_weights(): pl.pallas_call(weight_kernel, out_shape=[jax.ShapeDtypeStruct((size,) + w...  123 us
    pallas_call x1, Pallas kernels, attend(): pl.pallas_call(attention_kernel, out_shape=jax.ShapeDtypeStruct((2, half,...  31.1 us
    pallas_call x2, Pallas kernels, swiglu_groups(): pl.pallas_call(expert_kernel, out_shape=jax.ShapeDtypeStruct((count, widt...  16.8 us
    ppermute x2, starting transfers between devices, swap_high(): return lax.ppermute(block, axis, [(i, count - 1 - i) for i in range(count)])  14.6 us
    all_to_all x1, starting transfers between devices, body(): lax.all_to_all(routed_result, 'ep', split_axis=0, concat_axis=0, tiled=True)  10.6 us
    ppermute x3, waiting for transfers between devices, body(): lax.ppermute(leaving, 'tp', [(i, (i + step) % tp_size) for i in range(tp_...  9.75 us
    all_to_all x1, starting transfers between devices, body(): lax.all_to_all(outgoing, 'ep', split_axis=0, concat_axis=0, tiled=True)  9.43 us
  transfers between devices with their start and end apart: 9, of which 3 were waited for; matrix products, arithmetic and copies ran while one was open for 7% of the time, Pallas kernels for 66%

profile of v1, /device:TPU:1, one launch (start us, length us, event | category | flops | bytes accessed | tf_op | source)
XLA Modules:
  0.0 257.3 jit_solution(3544871000660437822)
XLA Ops:
  7.2 0.0 copy-start
  7.2 0.0 copy-start.6
  7.2 0.0 copy-start.12
  7.2 0.0 copy-start.11
  7.2 0.0 all-gather.4.cloned.1.call-start
  7.3 0.7 all-gather.4.cloned.1.call-update
  7.9 0.0 all-gather.6.cloned.1.call-start
  8.0 1.5 fusion.3
  9.5 0.0 copy-start.13
  9.6 0.0 copy-start.14
  9.6 0.0 copy-start.15
  9.6 1.8 fusion.12
  11.4 0.0 copy-start.8
  11.4 0.0 copy-done.13
  11.4 0.0 copy-start.5
  11.4 0.0 copy-start.7
  11.5 0.5 convolution_convert_fusion.2
  11.9 0.7 pad_maximum_fusion
  12.6 0.0 all-gather.6.cloned.1.call-update
  12.7 9.2 %collective-permute-start = (bf16[256,128]{1,0:T(8,128)(2,1)S(1)}, bf16[256,128]{1,0:T(8,128)(2,1)S(1)}, u32[]{:S(2)}, u32[]{:S(2)}) collective-permute-start(bf16[256,128]{1,0:T(8,128)(2,1)S(1)} %get-tuple-element.30), channel_id=1, source_target_pairs={{0,252},{4,248},{8,244},{12,240},{16,236},{20,232},{24,228},{28,22... | collective-permute-start | bytes 196616 | tf_op jit(solution)/shard_map/ppermute | solution.py:27
  21.9 0.1 copy.41
  22.0 0.1 eq.42
  22.2 0.3 fusion.15
  22.5 0.1 convert_element_type.65
  22.6 0.1 copy.42
  22.7 0.1 fusion.25
  22.8 0.2 fusion.16
  23.0 0.2 fusion.18.rows_ref
  23.2 0.0 copy-start.3
  23.2 0.5 convolution_convert_fusion
  23.7 1.5 reshape.62
  25.1 0.0 collective-permute-done.high_ref
  25.1 9.4 %all-to-all-start = ((bf16[64,80,128]{2,1,0:T(8,128)(2,1)}), bf16[64,80,128]{2,1,0:T(8,128)(2,1)S(1)}, u32[]{:S(2)}, u32[]{:S(2)}) async-start(bf16[64,80,128]{2,1,0:T(8,128)(2,1)} %reshape.62), calls=%async_computation | async-start | bytes 2621440 | tf_op jit(solution)/shard_map/all_to_all | solution.py:325
  34.6 123.1 %gather_weights.1 = (bf16[4,2048,256]{2,1,0:T(8,128)(2,1)}, bf16[4,256,2048]{2,1,0:T(8,128)(2,1)}, bf16[4,2048,128]{2,1,0:T(8,128)(2,1)}, bf16[4,2048,128]{2,1,0:T(8,128)(2,1)}, bf16[4,128,2048]{2,1,0:T(8,128)(2,1)}) custom-call(bf16[2048,256]{1,0:T(8,128)(2,1)} %bitcast.39, bf16[256,2048]{1,0:T(8,128)(2,1)} %bitcast.40, bf16[2048,128]{1,0:T(8,128)(2,1)} %refs_2_.1, ...), custom_call_target="tpu_custom_call" | custom-call | bytes 300000000 | tf_op jit(solution)/shard_map/gather_weights/pallas_call | solution.py:253
  157.7 0.0 all-to-all-done
  157.7 1.5 reshape.63.rows_ref
  159.2 10.3 %routed.1 = bf16[320,2048]{1,0:T(8,128)(2,1)} custom-call(bf16[320,2048]{1,0:T(8,128)(2,1)} %reshape.63.rows_ref, bf16[4,2048,256]{2,1,0:T(8,128)(2,1)} %all-gather.4.cloned.1.call-done.gate_ref, bf16[4,2048,256]{2,1,0:T(8,128)(2,1)} %get-tuple-element.13.up_ref, bf16[4,256,2048]{2,1,0:T(8,128)(2,1)} %get-tuple-element.14.down_ref), custom_call_target="tpu_custom_call" | custom-call | flops 4026531840 | bytes 12582912 | tf_op jit(solution)/shard_map/routed/pallas_call | solution.py:140
  169.6 3.3 %reshape.64 = bf16[64,80,128]{2,1,0:T(8,128)(2,1)} reshape(bf16[320,2048]{1,0:T(8,128)(2,1)} %routed.1) | data formatting | bytes 2621440 | tf_op jit(solution)/shard_map/reshape | solution.py:337
  172.9 10.6 %all-to-all-start.1 = ((bf16[64,80,128]{2,1,0:T(8,128)(2,1)}), bf16[64,80,128]{2,1,0:T(8,128)(2,1)S(1)}, u32[]{:S(2)}, u32[]{:S(2)}) async-start(bf16[64,80,128]{2,1,0:T(8,128)(2,1)} %reshape.64), calls=%async_computation.1 | async-start | bytes 2621440 | tf_op jit(solution)/shard_map/all_to_all | solution.py:338
  183.5 0.1 copy.43.gain_ref
  183.7 0.0 copy-start.9
  183.7 0.0 copy-start.16
  183.7 6.5 %shared.1 = f32[128,2048]{1,0:T(8,128)} custom-call(bf16[128,2048]{1,0:T(8,128)(2,1)} %copy-done.3, bf16[4,2048,128]{2,1,0:T(8,128)(2,1)} %get-tuple-element.16.gate_ref, bf16[4,2048,128]{2,1,0:T(8,128)(2,1)} %get-tuple-element.17.up_ref, bf16[4,128,2048]{2,1,0:T(8,128)(2,1)} %get-tuple-element.18.down_ref), custom_call_target="tpu_custom_call" | custom-call | flops 805306368 | bytes 6291456 | tf_op jit(solution)/shard_map/shared/pallas_call | solution.py:140
  190.2 0.1 iota_compare_fusion
  190.2 0.0 all-gather.6.cloned.1.call-done
  190.3 0.1 broadcast_in_dim.10
  190.3 3.4 %copy-done.1 = bf16[32768,128]{1,0:T(8,128)(2,1)S(1)} copy-done((bf16[32768,128]{1,0:T(8,128)(2,1)S(1)}, bf16[32768,128]{1,0:T(8,128)(2,1)}, u32[]{:S(2)}) %copy-start.1) | copy-done | bytes 8388632
  193.7 31.1 %attend.1 = bf16[2,128,256]{2,1,0:T(8,128)(2,1)S(1)} custom-call(s32[1]{0:T(128)} %bitcast.2.rank_ref, bf16[256,128]{1,0:T(8,128)(2,1)S(1)} %get-tuple-element.29.low_ref, bf16[256,128]{1,0:T(8,128)(2,1)S(1)} %collective-permute-done.high_ref, bf16[64,512,128]{2,1,0:T(8,128)(2,1)S(1)} %bitcast.35, f32[1,256]{1,0:T(1,128)S(1)} %bitcast.36, ...), custom_call_target="tpu_custom_call" | custom-call | flops 4294967296 | bytes 8388608 | tf_op jit(solution)/shard_map/attend/pallas_call | solution.py:98
  224.8 0.0 all-to-all-done.1
  224.8 1.0 copy-done.2
  225.9 5.3 %collective-permute-start.1 = (bf16[128,256]{1,0:T(8,128)(2,1)S(1)}, bf16[128,256]{1,0:T(8,128)(2,1)S(1)}, u32[]{:S(2)}, u32[]{:S(2)}) collective-permute-start(bf16[128,256]{1,0:T(8,128)(2,1)S(1)} %get-tuple-element.28), channel_id=1, source_target_pairs={{0,252},{4,248},{8,244},{12,240},{16,236},{20,232},{24,228},{28,22... | collective-permute-start | bytes 196616 | tf_op jit(solution)/shard_map/ppermute | solution.py:27
  231.2 2.4 reshape.68
  233.6 0.5 convolution_multiply_fusion.1
  234.1 0.0 collective-permute-done.1
  234.1 0.4 convolution_convert_fusion.1
  234.6 0.1 dynamic-slice_bitcast_fusion.2
  234.6 0.6 collective-permute-start.2
  235.3 1.4 collective-permute-start.3
  236.7 1.9 collective-permute-start.4
  238.6 1.3 fusion.2
  239.9 4.4 %collective-permute-done.2 = bf16[64,2048]{1,0:T(8,128)(2,1)S(1)} collective-permute-done((bf16[64,2048]{1,0:T(8,128)(2,1)S(1)}, bf16[64,2048]{1,0:T(8,128)(2,1)S(1)}, u32[]{:S(2)}, u32[]{:S(2)}) %collective-permute-start.2) | collective-permute-done | bytes 262176 | tf_op jit(solution)/shard_map/ppermute | solution.py:355
  244.3 4.4 %collective-permute-done.3 = bf16[64,2048]{1,0:T(8,128)(2,1)S(1)} collective-permute-done((bf16[64,2048]{1,0:T(8,128)(2,1)S(1)}, bf16[64,2048]{1,0:T(8,128)(2,1)S(1)}, u32[]{:S(2)}, u32[]{:S(2)}) %collective-permute-start.3) | collective-permute-done | bytes 262176 | tf_op jit(solution)/shard_map/ppermute | solution.py:355
  248.7 1.0 collective-permute-done.4
  249.6 0.8 fusion.24
  (29 shorter events, 0.1 us)
Async XLA Ops:
  7.2 226.9 %copy-start = (bf16[256,2048]{1,0:T(8,128)(2,1)S(1)}, bf16[256,2048]{1,0:T(8,128)(2,1)}, u32[]{:S(2)}) copy-start(bf16[256,2048]{1,0:T(8,128)(2,1)} %param.29) | copy-start | bytes 3145732
  7.2 2.3 copy-start.6
  7.2 2.3 copy-start.12
  7.2 2.3 copy-start.11
  7.2 152.0 %all-gather.4.cloned.1.call-start = ((), (), s32[]{:S(2)}) async-start(), calls=%async_computation.2 | async-start | bytes 5242880 | tf_op jit(solution)/shard_map/all_gather | solution.py:294
  7.9 182.3 %all-gather.6.cloned.1.call-start = ((), (), s32[]{:S(2)}) async-start(), calls=%async_computation.3 | async-start | bytes 8519680 | tf_op jit(solution)/shard_map/all_gather | solution.py:305
  9.5 1.9 copy-start.13
  9.6 1.9 copy-start.14
  9.6 1.9 copy-start.15
  11.4 10.6 %copy-start.8 = (s32[128,2]{0,1:T(2,128)S(1)}, s32[128,2]{0,1:T(2,128)}, u32[]{:S(2)}) copy-start(s32[128,2]{0,1:T(2,128)} %param.32) | copy-start | bytes 3076
  11.4 11.3 %copy-start.5 = (bf16[128,2048]{1,0:T(8,128)(2,1)S(1)}, bf16[128,2048]{1,0:T(8,128)(2,1)}, u32[]{:S(2)}) copy-start(bf16[128,2048]{1,0:T(8,128)(2,1)} %param.30) | copy-start | bytes 1572868
  11.4 11.5 %copy-start.7 = (f32[2048]{0:T(1024)S(1)}, f32[2048]{0:T(1024)}, u32[]{:S(2)}) copy-start(f32[2048]{0:T(1024)} %param.31) | copy-start | bytes 24580
  12.7 12.5 %collective-permute-start = (bf16[256,128]{1,0:T(8,128)(2,1)S(1)}, bf16[256,128]{1,0:T(8,128)(2,1)S(1)}, u32[]{:S(2)}, u32[]{:S(2)}) collective-permute-start(bf16[256,128]{1,0:T(8,128)(2,1)S(1)} %get-tuple-element.30), channel_id=1, source_target_pairs={{0,252},{4,248},{8,244},{12,240},{16,236},{20,232},{24,228},{28,22... | collective-permute-start | bytes 196616 | tf_op jit(solution)/shard_map/ppermute | solution.py:27
  23.2 2.0 copy-start.3
  25.1 132.6 %all-to-all-start = ((bf16[64,80,128]{2,1,0:T(8,128)(2,1)}), bf16[64,80,128]{2,1,0:T(8,128)(2,1)S(1)}, u32[]{:S(2)}, u32[]{:S(2)}) async-start(bf16[64,80,128]{2,1,0:T(8,128)(2,1)} %reshape.62), calls=%async_computation | async-start | bytes 2621440 | tf_op jit(solution)/shard_map/all_to_all | solution.py:325
  169.6 13.9 %copy-start.10 = (f32[128]{0:T(128)S(1)}, f32[128]{0:T(128)}, u32[]{:S(2)}) copy-start(f32[128]{0:T(128)} %param.28) | copy-start | bytes 1540
  172.9 51.9 %all-to-all-start.1 = ((bf16[64,80,128]{2,1,0:T(8,128)(2,1)}), bf16[64,80,128]{2,1,0:T(8,128)(2,1)S(1)}, u32[]{:S(2)}, u32[]{:S(2)}) async-start(bf16[64,80,128]{2,1,0:T(8,128)(2,1)} %reshape.64), calls=%async_computation.1 | async-start | bytes 2621440 | tf_op jit(solution)/shard_map/all_to_all | solution.py:338
  183.7 6.5 %copy-start.9 = (f32[128,2]{0,1:T(2,128)S(1)}, f32[128,2]{0,1:T(2,128)}, u32[]{:S(2)}) copy-start(f32[128,2]{0,1:T(2,128)} %param.33) | copy-start | bytes 3076
  183.7 6.6 %copy-start.16 = (f32[2]{0:T(128)S(1)}, f32[2]{0:T(128)}, u32[]{:S(2)}) copy-start(f32[2]{0:T(128)} %param.27) | copy-start | bytes 28
  190.3 3.4 %copy-start.1 = (bf16[32768,128]{1,0:T(8,128)(2,1)S(1)}, bf16[32768,128]{1,0:T(8,128)(2,1)}, u32[]{:S(2)}) copy-start(bf16[32768,128]{1,0:T(8,128)(2,1)} %all-gather.6.cloned.1.call-done) | copy-start | bytes 25165828
  224.8 1.1 copy-start.2
  225.9 8.2 %collective-permute-start.1 = (bf16[128,256]{1,0:T(8,128)(2,1)S(1)}, bf16[128,256]{1,0:T(8,128)(2,1)S(1)}, u32[]{:S(2)}, u32[]{:S(2)}) collective-permute-start(bf16[128,256]{1,0:T(8,128)(2,1)S(1)} %get-tuple-element.28), channel_id=1, source_target_pairs={{0,252},{4,248},{8,244},{12,240},{16,236},{20,232},{24,228},{28,22... | collective-permute-start | bytes 196616 | tf_op jit(solution)/shard_map/ppermute | solution.py:27
  234.1 4.5 %copy-start.4 = (f32[128,2048]{1,0:T(8,128)S(1)}, f32[128,2048]{1,0:T(8,128)}, u32[]{:S(2)}) copy-start(f32[128,2048]{1,0:T(8,128)} %shared.1) | copy-start | bytes 3145732
  234.6 9.6 %collective-permute-start.2 = (bf16[64,2048]{1,0:T(8,128)(2,1)S(1)}, bf16[64,2048]{1,0:T(8,128)(2,1)S(1)}, u32[]{:S(2)}, u32[]{:S(2)}) collective-permute-start(bf16[64,2048]{1,0:T(8,128)(2,1)S(1)} %get-tuple-element.22), channel_id=1, source_target_pairs={{0,1},{1,2},{2,3},{3,0},{4,5},{5,6},{6,7},{7,4},{8,9},{9,10},{10,1... | collective-permute-start | bytes 786440 | tf_op jit(solution)/shard_map/ppermute | solution.py:355
  235.3 13.4 %collective-permute-start.3 = (bf16[64,2048]{1,0:T(8,128)(2,1)S(1)}, bf16[64,2048]{1,0:T(8,128)(2,1)S(1)}, u32[]{:S(2)}, u32[]{:S(2)}) collective-permute-start(bf16[64,2048]{1,0:T(8,128)(2,1)S(1)} %get-tuple-element.24), channel_id=1, source_target_pairs={{0,2},{1,3},{2,0},{3,1},{4,6},{5,7},{6,4},{7,5},{8,10},{9,11},{10,... | collective-permute-start | bytes 786440 | tf_op jit(solution)/shard_map/ppermute | solution.py:355
  236.7 12.9 %collective-permute-start.4 = (bf16[64,2048]{1,0:T(8,128)(2,1)S(1)}, bf16[64,2048]{1,0:T(8,128)(2,1)S(1)}, u32[]{:S(2)}, u32[]{:S(2)}) collective-permute-start(bf16[64,2048]{1,0:T(8,128)(2,1)S(1)} %get-tuple-element.23), channel_id=1, source_target_pairs={{0,3},{1,0},{2,1},{3,2},{4,7},{5,4},{6,5},{7,6},{8,11},{9,8},{10,9... | collective-permute-start | bytes 786440 | tf_op jit(solution)/shard_map/ppermute | solution.py:355
Sparse Core Ops, SparseCore 0:
  9.8 78.5 all-gather.3
  91.8 85.2 all-gather.5

commit v2 on v1

v2 whole, which is shorter than its diff:
```python
import jax
import jax.numpy as jnp
from jax import lax
from jax.experimental import pallas as pl
from jax.experimental.pallas import tpu as pltpu
from jax.sharding import PartitionSpec as P

HEAD = 64

EPS = 1e-06
NEG = -1e30
MESH = pl.DeviceIdType.MESH

SPAN = 2
NX = 4


def normalize(activations, scaling):
    values = activations.astype(jnp.float32)
    factor = lax.rsqrt(jnp.mean(values * values, axis=-1, keepdims=True) + EPS)
    return (values * factor * scaling).astype(jnp.bfloat16)


def attention(rank, shards, rows, high_ref, low_ref, kv_ref, lam_ref, gain_ref, results, query, maxima, totals, weighted):
    half = rows // 2
    span_keys = SPAN * rows
    zeros = jnp.zeros((HEAD, 2 * half), jnp.bfloat16)
    for which, source in enumerate((low_ref, high_ref)):
        first = jnp.concatenate([source[0:HEAD], source[HEAD : 2 * HEAD]], axis=1)
        second = jnp.concatenate([source[2 * HEAD : 3 * HEAD], source[3 * HEAD : 4 * HEAD]], axis=1)
        query[which, 0, 0:HEAD] = first
        query[which, 0, HEAD : 2 * HEAD] = zeros
        query[which, 1, 0:HEAD] = zeros
        query[which, 1, HEAD : 2 * HEAD] = second

    def block(which, chip, masked, query_start):
        keys = kv_ref[chip, :, 0:rows, :].reshape(span_keys, 2 * HEAD)
        values = [kv_ref[chip, i, rows + j * half : rows + (j + 1) * half, :] for i in range(SPAN) for j in range(2)]
        values = jnp.concatenate(values, axis=1)
        if masked:
            key_pos = chip * span_keys + lax.broadcasted_iota(jnp.int32, (span_keys, 2 * half), 0)
            lane = lax.broadcasted_iota(jnp.int32, (span_keys, 2 * half), 1)
            query_pos = query_start + jnp.where(lane >= half, lane - half, lane)
            visible = key_pos <= query_pos
        for m in range(2):
            scores = jnp.dot(keys, query[which, m], preferred_element_type=jnp.float32)
            if masked:
                scores = jnp.where(visible, scores, NEG)
            earlier = maxima[which, m]
            latest = jnp.maximum(earlier, jnp.max(scores, axis=0, keepdims=True))
            shrink = jnp.exp(earlier - latest)
            weights = jnp.exp(scores - latest)
            if masked:
                weights = jnp.where(visible, weights, 0.0)
            totals[which, m] = totals[which, m] * shrink + jnp.sum(weights, axis=0, keepdims=True)
            product = jnp.dot(values, weights.astype(jnp.bfloat16), preferred_element_type=jnp.float32)
            weighted[which, m] = weighted[which, m] * shrink + product
            maxima[which, m] = latest

    for which in (1, 0):
        maxima[which] = jnp.full(maxima.shape[1:], NEG, jnp.float32)
        totals[which] = jnp.zeros(totals.shape[1:], jnp.float32)
        weighted[which] = jnp.zeros(weighted.shape[1:], jnp.float32)
        full = rank if which == 0 else shards - 1 - rank
        steps = full // SPAN

        def step(i, carry, which=which):
            block(which, i, False, 0)
            return carry

        lax.fori_loop(0, steps, step, 0)
        block(which, steps, True, full * rows + which * half)
        mixed = [weighted[which, m] / totals[which, m] for m in range(2)]
        combined = mixed[0] - lam_ref[...] * mixed[1]
        factor = lax.rsqrt(jnp.mean(combined * combined, axis=0, keepdims=True) + EPS)
        normed = combined * factor * gain_ref[...]
        for head in range(2):
            part = normed[:, head * half : (head + 1) * half]
            results[which][0:half, head * 128 : (head + 1) * 128] = part.T.astype(jnp.bfloat16)


def expert_kernel(rows_ref, gate_ref, up_ref, down_ref, out_ref, total):
    group = pl.program_id(0)
    rows = rows_ref[...]
    gated = jnp.dot(rows, gate_ref[0], preferred_element_type=jnp.float32)
    lifted = jnp.dot(rows, up_ref[0], preferred_element_type=jnp.float32)
    hidden = (gated / (1.0 + jnp.exp(-gated)) * lifted).astype(jnp.bfloat16)
    part = jnp.dot(hidden, down_ref[0], preferred_element_type=jnp.float32)
    part = part.astype(jnp.bfloat16).astype(jnp.float32)

    @pl.when(group == 0)
    def _():
        total[...] = part

    @pl.when(group > 0)
    def _():
        total[...] += part

    @pl.when(group == pl.num_programs(0) - 1)
    def _():
        out_ref[...] = total[...].astype(out_ref.dtype)


def swiglu_groups(rows, gate, up, down, kind, name):
    groups, width, hidden = gate.shape
    count = rows.shape[0]
    return pl.pallas_call(
        expert_kernel,
        out_shape=jax.ShapeDtypeStruct((count, width), kind),
        grid=(groups,),
        in_specs=[
            pl.BlockSpec((count, width), lambda g: (0, 0)),
            pl.BlockSpec((1, width, hidden), lambda g: (g, 0, 0)),
            pl.BlockSpec((1, width, hidden), lambda g: (g, 0, 0)),
            pl.BlockSpec((1, hidden, width), lambda g: (g, 0, 0)),
        ],
        out_specs=pl.BlockSpec((count, width), lambda g: (0, 0)),
        scratch_shapes=[pltpu.VMEM((count, width), jnp.float32)],
        cost_estimate=pl.CostEstimate(flops=groups * count * width * hidden * 6, bytes_accessed=groups * width * hidden * 6, transcendentals=groups * count * hidden),
        compiler_params=pltpu.CompilerParams(vmem_limit_bytes=60 * 1024 * 1024),
        name=name,
    )(rows, gate, up, down)


def send(source, target, send_sem, recv_sem, peer):
    copy = pltpu.make_async_remote_copy(
        src_ref=source, dst_ref=target, send_sem=send_sem, recv_sem=recv_sem, device_id=peer, device_id_type=MESH
    )
    copy.start()
    return copy


def greet(peers):
    barrier = pltpu.get_barrier_semaphore()
    for peer in peers:
        pl.semaphore_signal(barrier, inc=1, device_id=peer, device_id_type=MESH)
    pl.semaphore_wait(barrier, len(peers))


class Ring:
    def __init__(self, sources, targets, share, sems):
        self.sources, self.targets, self.share = sources, targets, share
        self.send_own, self.recv_own, self.send_on, self.recv_on, self.local = sems
        self.size, self.me = lax.axis_size("tp"), lax.axis_index("tp")
        self.at_right = lax.rem(self.me + 1, self.size)
        self.at_left = lax.rem(self.me + self.size - 1, self.size)
        self.sides = ({"tp": self.at_right}, {"tp": self.at_left})
        self.owners = (self.at_left, self.at_right)
        self.items = range(len(sources))

    def span_of(self, i):
        rows = self.sources[i].shape[0]
        return (rows, 0) if self.share is None else (rows // 2, self.share * (rows // 2))

    def piece(self, ref, i, part):
        rows, start = self.span_of(i)
        return ref.at[pl.ds(start + part * (rows // 2), rows // 2)]

    def whole(self, ref, i):
        rows, start = self.span_of(i)
        return ref.at[pl.ds(start, rows)]

    def start(self):
        self.own, self.onward, self.kept = {}, {}, []
        for order in range(2):
            for i in self.items:
                for side in range(2):
                    part = side if order == 0 else 1 - side
                    self.own[side, order, i] = send(
                        self.piece(self.sources[i], i, part),
                        self.piece(self.targets[i].at[self.me], i, part),
                        self.send_own.at[side, order, i],
                        self.recv_own.at[side, order, i],
                        self.sides[side],
                    )
        for i in self.items:
            copy = pltpu.make_async_copy(self.sources[i], self.targets[i].at[self.me], self.local.at[i])
            copy.start()
            self.kept.append(copy)

    def pass_on(self):
        for i in self.items:
            for side in range(2):
                self.own[side, 0, i].wait_recv()
                view = self.piece(self.targets[i].at[self.owners[side]], i, side)
                self.onward[side, i] = send(
                    view, view, self.send_on.at[side, i], self.recv_on.at[side, i], self.sides[side]
                )

    def finish_sends(self):
        for copy in self.kept:
            copy.wait()
        for i in self.items:
            for side in range(2):
                self.own[side, 0, i].wait_send()
                self.own[side, 1, i].wait_send()
                self.onward[side, i].wait_send()


def ring_sems(count):
    dma = pltpu.SemaphoreType.DMA
    return [dma((2, 2, count)), dma((2, 2, count)), dma((2, count)), dma((2, count)), dma((count,))]


class Spread:
    def __init__(self, sources, targets, x, core, tp_peers, across, other, sems):
        self.sources, self.targets, self.x, self.core = sources, targets, x, core
        self.tp_peers, self.across, self.other = tp_peers, across, other
        self.send_tp, self.recv_tp, self.send_x, self.recv_x, self.send_pair, self.recv_pair, self.local = sems
        self.me, self.size = lax.axis_index("tp"), lax.axis_size("tp")
        self.items = range(len(sources))

    def piece(self, ref, i):
        rows = self.sources[i].shape[0] // (2 * NX)
        return ref.at[pl.ds((self.core * NX + self.x) * rows, rows)]

    def start(self):
        self.first, self.kept = [], []
        for i in self.items:
            for k in range(1, self.size):
                target = self.piece(self.targets[i].at[self.me], i)
                sems = self.send_tp.at[k - 1, i], self.recv_tp.at[k - 1, i]
                self.first.append(send(self.piece(self.sources[i], i), target, *sems, self.tp_peers[k - 1]))
            copy = pltpu.make_async_copy(self.sources[i], self.targets[i].at[self.me], self.local.at[i])
            copy.start()
            self.kept.append(copy)

    def along_x(self):
        self.second = []
        for copy in self.first:
            copy.wait_recv()
        for i in self.items:
            for k in range(1, self.size):
                view = self.piece(self.targets[i].at[lax.rem(self.me + k, self.size)], i)
                for j, peer in enumerate(self.across):
                    sems = self.send_x.at[j, k - 1, i], self.recv_x.at[j, k - 1, i]
                    self.second.append(send(view, view, *sems, peer))

    def to_other(self):
        self.third = []
        for copy in self.second:
            copy.wait_recv()
        for i in self.items:
            rows = self.sources[i].shape[0] // 2
            for k in range(1, self.size):
                owner = lax.rem(self.me + k, self.size)
                view = self.targets[i].at[owner, pl.ds(self.core * rows, rows)]
                sems = self.send_pair.at[k - 1, i], self.recv_pair.at[k - 1, i]
                self.third.append(send(view, view, *sems, self.other))

    def finish(self):
        for copy in self.kept:
            copy.wait()
        for copy in self.third:
            copy.wait_recv()
        for copy in self.first + self.second + self.third:
            copy.wait_send()


def spread_sems(peers, count):
    dma = pltpu.SemaphoreType.DMA
    tp, along = (peers, count), (NX - 1, peers, count)
    return [dma(tp), dma(tp), dma(along), dma(along), dma(tp), dma(tp), dma((count,))]


def attend_kernel(
    up_ref,
    down_ref,
    shared_gate_ref,
    shared_up_ref,
    shared_down_ref,
    low_ref,
    high_ref,
    block_ref,
    lam_ref,
    gain_ref,
    up_out,
    down_out,
    shared_gate_out,
    shared_up_out,
    shared_down_out,
    out_ref,
    kv_ref,
    swapped,
    high_part,
    high_back,
    query,
    maxima,
    totals,
    weighted,
    send_x,
    recv_x,
    send_z,
    recv_z,
    send_pair,
    recv_pair,
    send_query,
    recv_query,
    send_back,
    recv_back,
    block_sem,
    *sems,
):
    count = lax.axis_size("ep")
    depth = count // (2 * NX)
    place = lax.axis_index("ep")
    core = lax.rem(place, 2)
    chip = lax.div(place, 2)
    x, z = lax.rem(chip, NX), lax.div(chip, NX)

    def at(zz, xx, cc):
        return {"ep": (zz * NX + xx) * 2 + cc}

    other = at(z, x, 1 - core)
    mirror = {"ep": count - 1 - place}
    across = [at(z, lax.rem(x + k, NX), core) for k in (1, 3, 2)]
    up, down = at(lax.rem(z + 1, depth), x, core), at(lax.rem(z + depth - 1, depth), x, core)
    ring = Ring((up_ref, down_ref), (up_out, down_out), None, sems[:5])
    opposite = {"tp": lax.rem(ring.me + 2, ring.size)}
    sources = (shared_gate_ref, shared_up_ref, shared_down_ref)
    targets = (shared_gate_out, shared_up_out, shared_down_out)
    tp_peers = (ring.sides[1], opposite, ring.sides[0])
    spread = Spread(sources, targets, x, core, tp_peers, across, other, sems[5:])
    greet(ring.sides + (opposite, other, mirror, up, down) + tuple(across))

    own_view = kv_ref.at[chip, core]
    along_x = [send(block_ref, own_view, send_x.at[k], recv_x.at[k], across[k]) for k in range(3)]
    own_block = pltpu.make_async_copy(block_ref, own_view, block_sem)
    own_block.start()
    asked = send(high_ref, swapped, send_query, recv_query, mirror)
    spread.start()
    ring.start()
    own_block.wait()
    for copy in along_x:
        copy.wait_recv()

    def level(zz, start, size):
        return kv_ref.at[pl.ds(zz * NX + start, size), core]

    pairs, along_z = [], []

    def to_other(zz, start, size, k):
        view = level(zz, start, size)
        pairs.append(send(view, view, send_pair.at[k], recv_pair.at[k], other))

    last = depth // 2
    for s in range(1, last + 1):
        parts = ((0, NX), (0, NX)) if s < last else ((0, NX // 2), (NX // 2, NX // 2))
        steps = []
        for way, peer in enumerate((up, down)):
            zz = lax.rem(z + (depth - s + 1 if way == 0 else s - 1), depth)
            view = level(zz, *parts[way])
            steps.append(send(view, view, send_z.at[s - 1, way], recv_z.at[s - 1, way], peer))
        if s == 1:
            to_other(z, 0, NX, 0)
        for way in range(2):
            steps[way].wait_recv()
            zz = lax.rem(z + (depth - s if way == 0 else s), depth)
            to_other(zz, *parts[way], 2 * s - 1 + way)
        along_z += steps
        if s == 2:
            spread.along_x()
    ring.pass_on()
    spread.to_other()
    for copy in pairs:
        copy.wait_recv()
    asked.wait_recv()

    rows = block_ref.shape[0] // 2
    results = (out_ref, high_part)
    attention(place, count, rows, swapped, low_ref, kv_ref, lam_ref, gain_ref, results, query, maxima, totals, weighted)
    answer = send(high_part, high_back, send_back, recv_back, mirror)

    for copy in along_x + along_z + pairs + [asked, answer]:
        copy.wait_send()
    answer.wait_recv()
    out_ref[rows // 2 :, :] = high_back[...]
    spread.finish()
    for i in ring.items:
        for side in range(2):
            ring.own[side, 1, i].wait_recv()
            ring.onward[side, i].wait_recv()
    ring.finish_sends()


def attend(weights, low, high, block, lambdas, head_gain):
    size = lax.axis_size("tp")
    count = lax.axis_size("ep")
    half = block.shape[0] // 4
    value_dim = head_gain.shape[0]
    lam = jnp.repeat(lambdas, half).reshape(1, 2 * half)
    vmem = pl.BlockSpec(memory_space=pltpu.VMEM)
    hbm = pl.BlockSpec(memory_space=pltpu.HBM)
    dma = pltpu.SemaphoreType.DMA
    steps = count // (4 * NX)
    return pl.pallas_call(
        attend_kernel,
        out_shape=[jax.ShapeDtypeStruct((size,) + w.shape, w.dtype) for w in weights]
        + [jax.ShapeDtypeStruct((2 * half, 2 * value_dim), jnp.bfloat16)],
        in_specs=[hbm] * 5 + [vmem] * 5,
        out_specs=[hbm] * 5 + [vmem],
        scratch_shapes=[
            pltpu.VMEM((count // 2, 2) + block.shape, block.dtype),
            pltpu.VMEM(high.shape, high.dtype),
            pltpu.VMEM((half, 2 * value_dim), jnp.bfloat16),
            pltpu.VMEM((half, 2 * value_dim), jnp.bfloat16),
            pltpu.VMEM((2, 2, 2 * HEAD, 2 * half), jnp.bfloat16),
            pltpu.VMEM((2, 2, 1, 2 * half), jnp.float32),
            pltpu.VMEM((2, 2, 1, 2 * half), jnp.float32),
            pltpu.VMEM((2, 2, value_dim, 2 * half), jnp.float32),
            dma((3,)),
            dma((3,)),
            dma((steps, 2)),
            dma((steps, 2)),
            dma((2 * steps + 1,)),
            dma((2 * steps + 1,)),
            dma,
            dma,
            dma,
            dma,
            dma,
        ]
        + ring_sems(2)
        + spread_sems(size - 1, 3),
        cost_estimate=pl.CostEstimate(flops=0, bytes_accessed=300_000_000, transcendentals=0),
        compiler_params=pltpu.CompilerParams(collective_id=0, has_side_effects=True, vmem_limit_bytes=60 * 1024 * 1024),
        name="attend",
    )(*weights, low, high, block, lam, head_gain.reshape(value_dim, 1))


def body(
    mixer_input,
    mixer_gain,
    query_one,
    query_two,
    key_one,
    key_two,
    value_weight,
    lambdas,
    head_gain,
    output_weight,
    expert_input,
    expert_gain,
    routes,
    route_weight,
    expert_gate,
    expert_up,
    expert_down,
    shared_gate,
    shared_up,
    shared_down,
):
    ep_size = lax.axis_size("ep")
    tp_size = lax.axis_size("tp")
    ep_rank = lax.axis_index("ep")
    mixer_rows, model_width = mixer_input.shape
    half_rows = mixer_rows // 2
    token_rows = expert_input.shape[0]

    gate_all = lax.all_gather(expert_gate[0], "tp")

    normed = normalize(mixer_input, mixer_gain)
    query_cols = query_one.shape[1]
    turned_weight = jnp.concatenate([query_one, query_two, value_weight], axis=1)
    turned = lax.dot_general(turned_weight, normed, (((0,), (1,)), ((), ())), preferred_element_type=jnp.float32)
    keys = jnp.dot(normed, jnp.concatenate([key_one, key_two], axis=1), preferred_element_type=jnp.float32)
    keys = keys.astype(jnp.bfloat16)
    queries = (turned[: 2 * query_cols].astype(jnp.bfloat16) * HEAD ** (-0.5)).astype(jnp.bfloat16)
    values = turned[2 * query_cols :].astype(jnp.bfloat16)
    key_values = jnp.concatenate([keys, values[:, :half_rows], values[:, half_rows:]], axis=0)

    normed_experts = normalize(expert_input, expert_gain)
    expert_count = expert_gate.shape[0] * ep_size
    top_count = routes.shape[1]
    capacity = max(2, 5 * token_rows * top_count // (4 * expert_count))
    slot_count = expert_count * capacity
    flat_routes = routes.reshape(-1)
    onehot = (flat_routes[:, None] == jnp.arange(expert_count, dtype=jnp.int32)[None, :]).astype(jnp.bfloat16)
    before = jnp.tril(jnp.ones((token_rows * top_count, token_rows * top_count), jnp.bfloat16), -1)
    counts = jnp.dot(before, onehot, preferred_element_type=jnp.float32)
    slot_place = jnp.sum(counts * onehot, axis=1).astype(jnp.int32)
    slot_ids = (flat_routes * capacity + slot_place).reshape(token_rows, top_count)
    slot_match = jnp.arange(slot_count, dtype=jnp.int32)[:, None, None] == slot_ids[None, :, :]
    select = jnp.any(slot_match, axis=2).astype(jnp.bfloat16)
    outgoing = jnp.dot(select, normed_experts, preferred_element_type=jnp.float32).astype(jnp.bfloat16)
    lines = slot_count // ep_size * model_width // 128
    outgoing = outgoing.reshape(ep_size, lines, 128)
    received = lax.all_to_all(outgoing, "ep", split_axis=0, concat_axis=0, tiled=True)

    weights = (expert_up[0], expert_down[0], shared_gate, shared_up, shared_down)
    up_all, down_all, *shared_weights, head_rows = attend(
        weights, queries[:, :half_rows], queries[:, half_rows:], key_values, lambdas, head_gain
    )

    slot_rows = received.reshape(slot_count, model_width)
    routed_result = swiglu_groups(slot_rows, gate_all, up_all, down_all, jnp.bfloat16, "routed")
    routed_result = routed_result.reshape(ep_size, lines, 128)

    normed_again, head_rows, routed_result = lax.optimization_barrier((normed_experts, head_rows, routed_result))
    returned = lax.all_to_all(routed_result, "ep", split_axis=0, concat_axis=0, tiled=True)
    shared_result = swiglu_groups(normed_again, *shared_weights, jnp.float32, "shared")
    partial = jnp.dot(head_rows, output_weight, preferred_element_type=jnp.float32).astype(jnp.bfloat16)
    partial = partial.reshape(tp_size, mixer_rows // tp_size, model_width)
    tp_rank = lax.axis_index("tp")
    mixer_sum = lax.dynamic_index_in_dim(partial, tp_rank, 0, keepdims=False).astype(jnp.float32)
    for step in range(1, tp_size):
        leaving = lax.dynamic_index_in_dim(partial, lax.rem(tp_rank + step, tp_size), 0, keepdims=False)
        part = lax.ppermute(leaving, "tp", [(i, (i + step) % tp_size) for i in range(tp_size)])
        mixer_sum = mixer_sum + part.astype(jnp.float32)
    mixer_output = mixer_sum.astype(jnp.bfloat16)

    returned, mixer_output, shared_result = lax.optimization_barrier((returned, mixer_output, shared_result))
    returned = returned.reshape(slot_count, model_width)
    picks = slot_ids[:, :, None] == jnp.arange(slot_count, dtype=jnp.int32)[None, None, :]
    picks = picks.astype(jnp.bfloat16)
    routed_total = jnp.zeros((token_rows, model_width), jnp.float32)
    for k in range(top_count):
        picked = jnp.dot(picks[:, k], returned, preferred_element_type=jnp.float32)
        routed_total = routed_total + picked * route_weight[:, k : k + 1]
    expert_output = (routed_total + shared_result).astype(jnp.bfloat16)
    return (mixer_output, expert_output)


def solution(mesh):
    in_specs = (
        P("ep", None),
        P(),
        P(None, "tp"),
        P(None, "tp"),
        P(None, "tp"),
        P(None, "tp"),
        P(None, "tp"),
        P("tp"),
        P(),
        P("tp", None),
        P(("ep", "tp"), None),
        P(),
        P(("ep", "tp"), None),
        P(("ep", "tp"), None),
        P("ep", None, "tp"),
        P("ep", None, "tp"),
        P("ep", "tp", None),
        P(None, "tp"),
        P(None, "tp"),
        P("tp", None),
    )
    out_specs = (P(("ep", "tp"), None), P(("ep", "tp"), None))
    return jax.shard_map(body, mesh=mesh, in_specs=in_specs, out_specs=out_specs, check_vma=False)
```

time: 258 us -> 222 us (0.86)
  Pallas kernels: 171 us -> 138 us
  starting transfers between devices: 38.6 us -> 23.9 us
  waiting for transfers between devices: 10.5 us -> 23.9 us
    pallas_call x2 -> x1, Pallas kernels: 154 us -> 121 us  [attend(): pl.pallas_call(attend_kernel, out_shape=[jax.ShapeDtypeStruct((size,) + w...]
    all_to_all x1, waiting for transfers between devices: 0.01 us -> 15.1 us  [body(): lax.all_to_all(routed_result, 'ep', split_axis=0, concat_axis=0, tiled=True)]
    ppermute x2 -> x0, starting transfers between devices: 14.6 us -> none  [swap_high(): return lax.ppermute(block, axis, [(i, count - 1 - i) for i in range(count)])]
    unnamed x35 -> x27, local copies, waits for them, and re-layouts: 4.63 us -> 0.86 us
    all_to_all x1, starting transfers between devices: 9.43 us -> 13.1 us  [body(): lax.all_to_all(outgoing, 'ep', split_axis=0, concat_axis=0, tiled=True)]
  transfers between devices with their start and end apart: 9 -> 6, of which waited for: 3 -> 3; matrix products, arithmetic and copies ran while one was open for 7% -> 6% of each run, Pallas kernels for 66% -> 58%
where the time goes in v2:
time: 222 us; the launch traced here: 221 us
  Pallas kernels  138 us (62%)
  starting transfers between devices  23.9 us (11%)
  waiting for transfers between devices  23.9 us (11%)
  between operations  14.3 us (6%)
  local copies, waits for them, and re-layouts  11.9 us (5%)
  matrix products  5.76 us (3%)
  other arithmetic  4.05 us (2%)
    pallas_call x1, Pallas kernels, attend(): pl.pallas_call(attend_kernel, out_shape=[jax.ShapeDtypeStruct((size,) + w...  121 us
    pallas_call x2, Pallas kernels, swiglu_groups(): pl.pallas_call(expert_kernel, out_shape=jax.ShapeDtypeStruct((count, widt...  16.7 us
    all_to_all x1, waiting for transfers between devices, body(): lax.all_to_all(routed_result, 'ep', split_axis=0, concat_axis=0, tiled=True)  15.1 us
    all_to_all x1, starting transfers between devices, body(): lax.all_to_all(outgoing, 'ep', split_axis=0, concat_axis=0, tiled=True)  13.1 us
    all_to_all x1, starting transfers between devices, body(): lax.all_to_all(routed_result, 'ep', split_axis=0, concat_axis=0, tiled=True)  8.39 us
    ppermute x3, waiting for transfers between devices, body(): lax.ppermute(leaving, 'tp', [(i, (i + step) % tp_size) for i in range(tp_...  8.14 us
  transfers between devices with their start and end apart: 6, of which 3 were waited for; matrix products, arithmetic and copies ran while one was open for 6% of the time, Pallas kernels for 58%

profile of v2, /device:TPU:1, one launch (start us, length us, event | category | flops | bytes accessed | tf_op | source)
XLA Modules:
  0.0 221.3 jit_solution(8380678549822807659)
XLA Ops:
  7.2 0.0 copy-start
  7.2 0.0 copy-start.3
  7.2 0.0 copy-start.6
  7.2 0.0 all-gather.2.cloned.1.call-start
  7.2 0.7 all-gather.2.cloned.1.call-update
  7.9 0.8 copy.42
  8.7 0.1 eq.42
  8.9 0.3 fusion.15
  9.2 0.1 convert_element_type.70
  9.3 0.1 copy.43
  9.4 0.7 multiply_add_fusion
  10.1 1.2 fusion.16
  11.4 0.0 copy-done.3
  11.4 0.0 copy-done.6
  11.4 0.2 fusion.18.rows_ref
  11.6 0.0 copy-start.1
  11.6 0.5 convolution_convert_fusion
  12.1 0.0 copy-start.8
  12.1 1.5 reshape.60
  13.6 0.0 copy-done.1
  13.6 0.0 copy-start.4
  13.6 13.1 %all-to-all-start = ((bf16[64,80,128]{2,1,0:T(8,128)(2,1)}), bf16[64,80,128]{2,1,0:T(8,128)(2,1)S(1)}, u32[]{:S(2)}, u32[]{:S(2)}) async-start(bf16[64,80,128]{2,1,0:T(8,128)(2,1)} %reshape.60), calls=%async_computation | async-start | bytes 2621440 | tf_op jit(solution)/shard_map/all_to_all | solution.py:488
  26.7 0.0 copy-done.8
  26.7 0.7 copy.41.gain_ref
  27.4 0.0 copy-done.4
  27.4 0.3 fusion.3
  27.7 0.0 copy-done.11
  27.7 0.0 copy-start.9
  27.7 0.0 copy-start.10
  27.8 2.3 %fusion.12 = bf16[384,256]{1,0:T(8,128)(2,1)S(1)} fusion(bf16[2048,128]{1,0:T(8,128)(2,1)} %param.26, bf16[2048,128]{1,0:T(8,128)(2,1)} %param.23, bf16[2048,128]{1,0:T(8,128)(2,1)} %param.22, bf16[256,2048]{1,0:T(8,128)(2,1)S(1)} %copy-done.4, f32[2048]{0:T(1024)S(1)} %copy-done.11, f32[256]{0:T(256)S(1)} %add_rsqrt_fusion), kind=kOutput, calls=%fused_computation.20 | convolution fusion | flops 409567232 | bytes 2827264 | tf_op jit(solution)/shard_map/dot_general | solution.py:465
  30.0 0.0 copy-start.12
  30.0 0.0 copy-done.9
  30.1 0.0 copy-done.10
  30.1 0.5 convolution_convert_fusion.2
  30.6 0.7 pad_maximum_fusion.block_ref
  31.3 0.7 fusion.40
  31.9 0.0 copy-done.12
  31.9 0.6 broadcast_in_dim.8
  32.5 120.8 %attend.1 = (bf16[4,2048,256]{2,1,0:T(8,128)(2,1)}, bf16[4,256,2048]{2,1,0:T(8,128)(2,1)}, bf16[4,2048,128]{2,1,0:T(8,128)(2,1)}, bf16[4,2048,128]{2,1,0:T(8,128...) custom-call(bf16[2048,256]{1,0:T(8,128)(2,1)} %bitcast.32, bf16[256,2048]{1,0:T(8,128)(2,1)} %bitcast.33, ...), custom_call_target="tpu_custom_call" | custom-call | bytes 300000000 | tf_op jit(solution)/shard_map/attend/pallas_call | solution.py:396
  153.4 0.0 all-to-all-done
  153.4 1.4 reshape.61.rows_ref
  154.8 10.2 %routed.1 = bf16[320,2048]{1,0:T(8,128)(2,1)} custom-call(bf16[320,2048]{1,0:T(8,128)(2,1)} %reshape.61.rows_ref, bf16[4,2048,256]{2,1,0:T(8,128)(2,1)} %all-gather.2.cloned.1.call-done.gate_ref, bf16[4,2048,256]{2,1,0:T(8,128)(2,1)} %get-tuple-element.15.up_ref, bf16[4,256,2048]{2,1,0:T(8,128)(2,1)} %get-tuple-element.16.down_ref), custom_call_target="tpu_custom_call" | custom-call | flops 4026531840 | bytes 12582912 | tf_op jit(solution)/shard_map/routed/pallas_call | solution.py:107
  165.0 3.3 %reshape.62 = bf16[64,80,128]{2,1,0:T(8,128)(2,1)} reshape(bf16[320,2048]{1,0:T(8,128)(2,1)} %routed.1) | data formatting | bytes 2621440 | tf_op jit(solution)/shard_map/reshape | solution.py:497
  168.4 8.4 %all-to-all-start.1 = ((bf16[64,80,128]{2,1,0:T(8,128)(2,1)}), bf16[64,80,128]{2,1,0:T(8,128)(2,1)}, u32[]{:S(2)}, u32[]{:S(2)}) async-start(bf16[64,80,128]{2,1,0:T(8,128)(2,1)} %reshape.62), calls=%async_computation.1 | async-start | bytes 2621440 | tf_op jit(solution)/shard_map/all_to_all | solution.py:500
  176.8 0.0 copy-start.7
  176.8 0.1 iota_compare_fusion
  176.9 0.0 copy-done
  176.9 0.0 copy-done.5
  176.9 0.4 convolution_convert_fusion.1
  177.3 0.1 dynamic-slice_bitcast_fusion.2
  177.4 1.6 collective-permute-start.2
  179.0 0.7 collective-permute-start.1
  179.7 0.1 collective-permute-start
  179.8 0.0 copy-done.7
  179.8 6.5 %shared.1 = f32[128,2048]{1,0:T(8,128)} custom-call(bf16[128,2048]{1,0:T(8,128)(2,1)} %copy-done.1, bf16[4,2048,128]{2,1,0:T(8,128)(2,1)} %get-tuple-element.20.gate_ref, bf16[4,2048,128]{2,1,0:T(8,128)(2,1)} %get-tuple-element.21.up_ref, bf16[4,128,2048]{2,1,0:T(8,128)(2,1)} %get-tuple-element.22.down_ref), custom_call_target="tpu_custom_call" | custom-call | flops 805306368 | bytes 6291456 | tf_op jit(solution)/shard_map/shared/pallas_call | solution.py:107
  186.3 0.0 collective-permute-done.2
  186.3 1.2 collective-permute-done.1
  187.5 6.9 %collective-permute-done = bf16[64,2048]{1,0:T(8,128)(2,1)S(1)} collective-permute-done((bf16[64,2048]{1,0:T(8,128)(2,1)S(1)}, bf16[64,2048]{1,0:T(8,128)(2,1)S(1)}, u32[]{:S(2)}, u32[]{:S(2)}) %collective-permute-start) | collective-permute-done | bytes 262176 | tf_op jit(solution)/shard_map/ppermute | solution.py:508
  194.4 0.8 fusion.24
  195.3 15.1 %all-to-all-done.1 = bf16[64,80,128]{2,1,0:T(8,128)(2,1)} async-done(((bf16[64,80,128]{2,1,0:T(8,128)(2,1)}), bf16[64,80,128]{2,1,0:T(8,128)(2,1)}, u32[]{:S(2)}, u32[]{:S(2)}) %all-to-all-start.1) | async-done | bytes 1310752 | tf_op jit(solution)/shard_map/all_to_all | solution.py:500
  210.3 2.4 %reshape.64 = bf16[320,2048]{1,0:T(8,128)(2,1)S(1)} reshape(bf16[64,80,128]{2,1,0:T(8,128)(2,1)} %all-to-all-done.1) | data formatting | bytes 2621440 | tf_op jit(solution)/shard_map/reshape | solution.py:513
  212.7 0.5 convolution_multiply_fusion.1
  213.2 0.0 copy-done.2
  213.2 1.3 fusion.2
  (12 shorter events, 0.1 us)
Async XLA Ops:
  7.2 169.7 %copy-start = (bf16[256,2048]{1,0:T(8,128)(2,1)S(1)}, bf16[256,2048]{1,0:T(8,128)(2,1)}, u32[]{:S(2)}) copy-start(bf16[256,2048]{1,0:T(8,128)(2,1)} %param.29) | copy-start | bytes 3145732
  7.2 4.2 %copy-start.3 = (bf16[128,2048]{1,0:T(8,128)(2,1)S(1)}, bf16[128,2048]{1,0:T(8,128)(2,1)}, u32[]{:S(2)}) copy-start(bf16[128,2048]{1,0:T(8,128)(2,1)} %param.30) | copy-start | bytes 1572868
  7.2 4.2 %copy-start.6 = (f32[2048]{0:T(1024)S(1)}, f32[2048]{0:T(1024)}, u32[]{:S(2)}) copy-start(f32[2048]{0:T(1024)} %param.31) | copy-start | bytes 24580
  7.2 147.6 %all-gather.2.cloned.1.call-start = ((), (), s32[]{:S(2)}) async-start(), calls=%async_computation.2 | async-start | bytes 5242880 | tf_op jit(solution)/shard_map/all_gather | solution.py:460
  11.6 2.0 copy-start.1
  12.1 14.6 %copy-start.8 = (f32[128]{0:T(128)S(1)}, f32[128]{0:T(128)}, u32[]{:S(2)}) copy-start(f32[128]{0:T(128)} %param.28) | copy-start | bytes 1540
  13.6 13.9 %copy-start.4 = (bf16[256,2048]{1,0:T(8,128)(2,1)S(1)}, bf16[256,2048]{1,0:T(8,128)(2,1)}, u32[]{:S(2)}) copy-start(bf16[256,2048]{1,0:T(8,128)(2,1)} %param.20) | copy-start | bytes 3145732
  13.6 14.2 %copy-start.11 = (f32[2048]{0:T(1024)S(1)}, f32[2048]{0:T(1024)}, u32[]{:S(2)}) copy-start(f32[2048]{0:T(1024)} %param.21) | copy-start | bytes 24580
  13.6 139.8 %all-to-all-start = ((bf16[64,80,128]{2,1,0:T(8,128)(2,1)}), bf16[64,80,128]{2,1,0:T(8,128)(2,1)S(1)}, u32[]{:S(2)}, u32[]{:S(2)}) async-start(bf16[64,80,128]{2,1,0:T(8,128)(2,1)} %reshape.60), calls=%async_computation | async-start | bytes 2621440 | tf_op jit(solution)/shard_map/all_to_all | solution.py:488
  27.7 2.3 %copy-start.9 = (bf16[2048,64]{0,1:T(8,128)(2,1)S(1)}, bf16[2048,64]{0,1:T(8,128)(2,1)}, u32[]{:S(2)}) copy-start(bf16[2048,64]{0,1:T(8,128)(2,1)} %param.25) | copy-start | bytes 786436
  27.7 2.3 %copy-start.10 = (bf16[2048,64]{0,1:T(8,128)(2,1)S(1)}, bf16[2048,64]{0,1:T(8,128)(2,1)}, u32[]{:S(2)}) copy-start(bf16[2048,64]{0,1:T(8,128)(2,1)} %param.24) | copy-start | bytes 786436
  30.0 1.9 copy-start.12
  165.0 11.8 %copy-start.5 = (bf16[256,256]{1,0:T(8,128)(2,1)S(1)}, bf16[256,256]{1,0:T(8,128)(2,1)}, u32[]{:S(2)}) copy-start(bf16[256,256]{1,0:T(8,128)(2,1)} %get-tuple-element.18) | copy-start | bytes 393220
  168.4 42.0 %all-to-all-start.1 = ((bf16[64,80,128]{2,1,0:T(8,128)(2,1)}), bf16[64,80,128]{2,1,0:T(8,128)(2,1)}, u32[]{:S(2)}, u32[]{:S(2)}) async-start(bf16[64,80,128]{2,1,0:T(8,128)(2,1)} %reshape.62), calls=%async_computation.1 | async-start | bytes 2621440 | tf_op jit(solution)/shard_map/all_to_all | solution.py:500
  176.8 3.0 %copy-start.7 = (f32[128,2]{0,1:T(2,128)S(1)}, f32[128,2]{0,1:T(2,128)}, u32[]{:S(2)}) copy-start(f32[128,2]{0,1:T(2,128)} %param.33) | copy-start | bytes 3076
  177.4 8.9 %collective-permute-start.2 = (bf16[64,2048]{1,0:T(8,128)(2,1)S(1)}, bf16[64,2048]{1,0:T(8,128)(2,1)S(1)}, u32[]{:S(2)}, u32[]{:S(2)}) collective-permute-start(bf16[64,2048]{1,0:T(8,128)(2,1)S(1)} %get-tuple-element.27), channel_id=1, source_target_pairs={{0,3},{1,0},{2,1},{3,2},{4,7},{5,4},{6,5},{7,6},{8,11},{9,8},{10,9... | collective-permute-start | bytes 786440 | tf_op jit(solution)/shard_map/ppermute | solution.py:508
  179.0 8.5 %collective-permute-start.1 = (bf16[64,2048]{1,0:T(8,128)(2,1)S(1)}, bf16[64,2048]{1,0:T(8,128)(2,1)S(1)}, u32[]{:S(2)}, u32[]{:S(2)}) collective-permute-start(bf16[64,2048]{1,0:T(8,128)(2,1)S(1)} %get-tuple-element.28), channel_id=1, source_target_pairs={{0,2},{1,3},{2,0},{3,1},{4,6},{5,7},{6,4},{7,5},{8,10},{9,11},{10,... | collective-permute-start | bytes 786440 | tf_op jit(solution)/shard_map/ppermute | solution.py:508
  179.7 14.8 %collective-permute-start = (bf16[64,2048]{1,0:T(8,128)(2,1)S(1)}, bf16[64,2048]{1,0:T(8,128)(2,1)S(1)}, u32[]{:S(2)}, u32[]{:S(2)}) collective-permute-start(bf16[64,2048]{1,0:T(8,128)(2,1)S(1)} %get-tuple-element.26), channel_id=1, source_target_pairs={{0,1},{1,2},{2,3},{3,0},{4,5},{5,6},{6,7},{7,4},{8,9},{9,10},{10,1... | collective-permute-start | bytes 786440 | tf_op jit(solution)/shard_map/ppermute | solution.py:508
  195.3 17.9 %copy-start.2 = (f32[128,2048]{1,0:T(8,128)S(1)}, f32[128,2048]{1,0:T(8,128)}, u32[]{:S(2)}) copy-start(f32[128,2048]{1,0:T(8,128)} %shared.1) | copy-start | bytes 3145732
Sparse Core Ops, SparseCore 0:
  9.8 79.2 all-gather.1

commit v3 on v2

--- a/solution.py
+++ b/solution.py
@@ -130,11 +130,19 @@
     return copy
 
 
-def greet(peers):
+def greet(peers, count):
     barrier = pltpu.get_barrier_semaphore()
+    place = lax.axis_index("ep")
     for peer in peers:
         pl.semaphore_signal(barrier, inc=1, device_id=peer, device_id_type=MESH)
-    pl.semaphore_wait(barrier, len(peers))
+
+    def one(k, carry):
+        peer = {"ep": lax.rem(place + k, count)}
+        pl.semaphore_signal(barrier, inc=1, device_id=peer, device_id_type=MESH)
+        return carry
+
+    lax.fori_loop(1, count, one, 0)
+    pl.semaphore_wait(barrier, len(peers) + count - 1)
 
 
 class Ring:
@@ -188,8 +196,6 @@
                 )
 
     def finish_sends(self):
-        for copy in self.kept:
-            copy.wait()
         for i in self.items:
             for side in range(2):
                 self.own[side, 0, i].wait_send()
@@ -264,22 +270,29 @@
 
 
 def attend_kernel(
+    gate_ref,
     up_ref,
     down_ref,
     shared_gate_ref,
     shared_up_ref,
     shared_down_ref,
+    leaving_ref,
     low_ref,
     high_ref,
     block_ref,
     lam_ref,
     gain_ref,
-    up_out,
-    down_out,
     shared_gate_out,
     shared_up_out,
     shared_down_out,
+    landed_ref,
+    routed_ref,
     out_ref,
+    gate_all,
+    up_all,
+    down_all,
+    landed,
+    total,
     kv_ref,
     swapped,
     high_part,
@@ -298,6 +311,8 @@
     recv_query,
     send_back,
     recv_back,
+    send_rows,
+    recv_rows,
     block_sem,
     *sems,
 ):
@@ -315,13 +330,13 @@
     mirror = {"ep": count - 1 - place}
     across = [at(z, lax.rem(x + k, NX), core) for k in (1, 3, 2)]
     up, down = at(lax.rem(z + 1, depth), x, core), at(lax.rem(z + depth - 1, depth), x, core)
-    ring = Ring((up_ref, down_ref), (up_out, down_out), None, sems[:5])
+    ring = Ring((gate_ref, up_ref, down_ref), (gate_all, up_all, down_all), None, sems[:5])
     opposite = {"tp": lax.rem(ring.me + 2, ring.size)}
     sources = (shared_gate_ref, shared_up_ref, shared_down_ref)
     targets = (shared_gate_out, shared_up_out, shared_down_out)
     tp_peers = (ring.sides[1], opposite, ring.sides[0])
     spread = Spread(sources, targets, x, core, tp_peers, across, other, sems[5:])
-    greet(ring.sides + (opposite, other, mirror, up, down) + tuple(across))
+    greet(ring.sides + (opposite,), count)
 
     own_view = kv_ref.at[chip, core]
     along_x = [send(block_ref, own_view, send_x.at[k], recv_x.at[k], across[k]) for k in range(3)]
@@ -361,6 +376,34 @@
         if s == 2:
             spread.along_x()
     ring.pass_on()
+
+    slots = leaving_ref.shape[0] // count
+
+    def rows_of(ref, owner):
+        return ref.at[pl.ds(pl.multiple_of(owner * slots, slots), slots)]
+
+    def row_copy(k):
+        peer = lax.rem(place + k, count)
+        return pltpu.make_async_remote_copy(
+            src_ref=rows_of(leaving_ref, peer),
+            dst_ref=rows_of(landed_ref, place),
+            send_sem=send_rows.at[k],
+            recv_sem=recv_rows.at[k],
+            device_id={"ep": peer},
+            device_id_type=MESH,
+        )
+
+    def start_rows(k, carry):
+        row_copy(k).start()
+        return carry
+
+    def wait_rows(k, carry):
+        row_copy(k).wait()
+        return carry
+
+    lax.fori_loop(1, count, start_rows, 0)
+    own_rows = pltpu.make_async_copy(rows_of(leaving_ref, place), rows_of(landed_ref, place), send_rows.at[0])
+    own_rows.start()
     spread.to_other()
     for copy in pairs:
         copy.wait_recv()
@@ -371,19 +414,49 @@
     attention(place, count, rows, swapped, low_ref, kv_ref, lam_ref, gain_ref, results, query, maxima, totals, weighted)
     answer = send(high_part, high_back, send_back, recv_back, mirror)
 
+    lax.fori_loop(1, count, wait_rows, 0)
+    own_rows.wait()
+    fetch = pltpu.make_async_copy(landed_ref, landed, recv_rows.at[0])
+    fetch.start()
     for copy in along_x + along_z + pairs + [asked, answer]:
         copy.wait_send()
     answer.wait_recv()
     out_ref[rows // 2 :, :] = high_back[...]
+    fetch.wait()
+
+    def group(owner, first):
+        tile = 256
+
+        def step(i, carry):
+            span = pl.ds(pl.multiple_of(i * tile, tile), tile)
+            some = landed[span, :]
+            gated = jnp.dot(some, gate_all[owner], preferred_element_type=jnp.float32)
+            lifted = jnp.dot(some, up_all[owner], preferred_element_type=jnp.float32)
+            hidden = (gated / (1.0 + jnp.exp(-gated)) * lifted).astype(jnp.bfloat16)
+            part = jnp.dot(hidden, down_all[owner], preferred_element_type=jnp.float32)
+            part = part.astype(jnp.bfloat16).astype(jnp.float32)
+            total[span, :] = part if first else total[span, :] + part
+            return carry
+
+        lax.fori_loop(0, landed.shape[0] // tile, step, 0)
+
+    for copy in ring.kept:
+        copy.wait()
+    group(ring.me, True)
+    for side in range(2):
+        for i in ring.items:
+            ring.own[side, 1, i].wait_recv()
+        group(ring.owners[side], False)
     spread.finish()
     for i in ring.items:
         for side in range(2):
-            ring.own[side, 1, i].wait_recv()
             ring.onward[side, i].wait_recv()
+    group(lax.rem(ring.me + 2, ring.size), False)
+    routed_ref[...] = total[...].astype(routed_ref.dtype)
     ring.finish_sends()
 
 
-def attend(weights, low, high, block, lambdas, head_gain):
+def attend(weights, leaving, low, high, block, lambdas, head_gain):
     size = lax.axis_size("tp")
     count = lax.axis_size("ep")
     half = block.shape[0] // 4
@@ -395,11 +468,15 @@
     steps = count // (4 * NX)
     return pl.pallas_call(
         attend_kernel,
-        out_shape=[jax.ShapeDtypeStruct((size,) + w.shape, w.dtype) for w in weights]
+        out_shape=[jax.ShapeDtypeStruct((size,) + w.shape, w.dtype) for w in weights[3:]]
+        + [jax.ShapeDtypeStruct(leaving.shape, leaving.dtype)] * 2
         + [jax.ShapeDtypeStruct((2 * half, 2 * value_dim), jnp.bfloat16)],
-        in_specs=[hbm] * 5 + [vmem] * 5,
-        out_specs=[hbm] * 5 + [vmem],
-        scratch_shapes=[
+        in_specs=[hbm] * 7 + [vmem] * 5,
+        out_specs=[hbm] * 4 + [vmem] * 2,
+        scratch_shapes=[pltpu.VMEM((size,) + w.shape, w.dtype) for w in weights[:3]]
+        + [
+            pltpu.VMEM(leaving.shape, leaving.dtype),
+            pltpu.VMEM(leaving.shape, jnp.float32),
             pltpu.VMEM((count // 2, 2) + block.shape, block.dtype),
             pltpu.VMEM(high.shape, high.dtype),
             pltpu.VMEM((half, 2 * value_dim), jnp.bfloat16),
@@ -418,14 +495,16 @@
             dma,
             dma,
             dma,
+            dma((count,)),
+            dma((count,)),
             dma,
         ]
-        + ring_sems(2)
+        + ring_sems(3)
         + spread_sems(size - 1, 3),
         cost_estimate=pl.CostEstimate(flops=0, bytes_accessed=300_000_000, transcendentals=0),
         compiler_params=pltpu.CompilerParams(collective_id=0, has_side_effects=True, vmem_limit_bytes=60 * 1024 * 1024),
         name="attend",
-    )(*weights, low, high, block, lam, head_gain.reshape(value_dim, 1))
+    )(*weights, leaving, low, high, block, lam, head_gain.reshape(value_dim, 1))
 
 
 def body(
@@ -457,8 +536,6 @@
     half_rows = mixer_rows // 2
     token_rows = expert_input.shape[0]
 
-    gate_all = lax.all_gather(expert_gate[0], "tp")
-
     normed = normalize(mixer_input, mixer_gain)
     query_cols = query_one.shape[1]
     turned_weight = jnp.concatenate([query_one, query_two, value_weight], axis=1)
@@ -480,21 +557,18 @@
     counts = jnp.dot(before, onehot, preferred_element_type=jnp.float32)
     slot_place = jnp.sum(counts * onehot, axis=1).astype(jnp.int32)
     slot_ids = (flat_routes * capacity + slot_place).reshape(token_rows, top_count)
-    slot_match = jnp.arange(slot_count, dtype=jnp.int32)[:, None, None] == slot_ids[None, :, :]
+    padded = -(-capacity // 8) * 8
+    leaving_ids = (flat_routes * padded + slot_place).reshape(token_rows, top_count)
+    slot_match = jnp.arange(expert_count * padded, dtype=jnp.int32)[:, None, None] == leaving_ids[None, :, :]
     select = jnp.any(slot_match, axis=2).astype(jnp.bfloat16)
     outgoing = jnp.dot(select, normed_experts, preferred_element_type=jnp.float32).astype(jnp.bfloat16)
+
+    weights = (expert_gate[0], expert_up[0], expert_down[0], shared_gate, shared_up, shared_down)
+    *shared_weights, _, routed_result, head_rows = attend(
+        weights, outgoing, queries[:, :half_rows], queries[:, half_rows:], key_values, lambdas, head_gain
+    )
     lines = slot_count // ep_size * model_width // 128
-    outgoing = outgoing.reshape(ep_size, lines, 128)
-    received = lax.all_to_all(outgoing, "ep", split_axis=0, concat_axis=0, tiled=True)
-
-    weights = (expert_up[0], expert_down[0], shared_gate, shared_up, shared_down)
-    up_all, down_all, *shared_weights, head_rows = attend(
-        weights, queries[:, :half_rows], queries[:, half_rows:], key_values, lambdas, head_gain
-    )
-
-    slot_rows = received.reshape(slot_count, model_width)
-    routed_result = swiglu_groups(slot_rows, gate_all, up_all, down_all, jnp.bfloat16, "routed")
-    routed_result = routed_result.reshape(ep_size, lines, 128)
+    routed_result = routed_result.reshape(ep_size, padded, model_width)[:, :capacity].reshape(ep_size, lines, 128)
 
     normed_again, head_rows, routed_result = lax.optimization_barrier((normed_experts, head_rows, routed_result))
     returned = lax.all_to_all(routed_result, "ep", split_axis=0, concat_axis=0, tiled=True)

time: 222 us -> 198 us (0.89)
  between operations: 14.3 us -> 0.93 us
  starting transfers between devices: 23.9 us -> 16.4 us
  waiting for transfers between devices: 23.9 us -> 20.5 us
  local copies, waits for them, and re-layouts: 11.9 us -> 9.1 us
    all_to_all x1 -> x0, starting transfers between devices: 13.1 us -> none  [body(): lax.all_to_all(outgoing, 'ep', split_axis=0, concat_axis=0, tiled=True)]
    pallas_call x1, Pallas kernels: 121 us -> 132 us  [attend(): pl.pallas_call(attend_kernel, out_shape=[jax.ShapeDtypeStruct((size,) + w...]
    pallas_call x2 -> x1, Pallas kernels: 16.7 us -> 6.49 us  [swiglu_groups(): pl.pallas_call(expert_kernel, out_shape=jax.ShapeDtypeStruct((count, widt...]
    all_to_all x1, starting transfers between devices: 8.39 us -> 12.2 us  [body(): lax.all_to_all(routed_result, 'ep', split_axis=0, concat_axis=0, tiled=True)]
    all_to_all x1, waiting for transfers between devices: 15.1 us -> 12.7 us  [body(): lax.all_to_all(routed_result, 'ep', split_axis=0, concat_axis=0, tiled=True)]
    reshape x3 -> x1, local copies, waits for them, and re-layouts: 6.24 us -> 4.11 us  [body(): routed_result.reshape(ep_size, padded, model_width)[:, :capacity]]
  transfers between devices with their start and end apart: 6 -> 4, of which waited for: 3 -> 3; matrix products, arithmetic and copies ran while one was open for 6% -> 1% of each run, Pallas kernels for 58% -> 3%
where the time goes in v3:
time: 198 us
  Pallas kernels  139 us (70%)
  waiting for transfers between devices  20.5 us (10%)
  starting transfers between devices  16.4 us (8%)
  local copies, waits for them, and re-layouts  9.1 us (5%)
  matrix products  7.5 us (4%)
  other arithmetic  4.6 us (2%)
    pallas_call x1, Pallas kernels, attend(): pl.pallas_call(attend_kernel, out_shape=[jax.ShapeDtypeStruct((size,) + w...  132 us
    all_to_all x1, waiting for transfers between devices, body(): lax.all_to_all(routed_result, 'ep', split_axis=0, concat_axis=0, tiled=True)  12.7 us
    all_to_all x1, starting transfers between devices, body(): lax.all_to_all(routed_result, 'ep', split_axis=0, concat_axis=0, tiled=True)  12.2 us
    ppermute x3, waiting for transfers between devices, body(): lax.ppermute(leaving, 'tp', [(i, (i + step) % tp_size) for i in range(tp_...  7.78 us
    pallas_call x1, Pallas kernels, swiglu_groups(): pl.pallas_call(expert_kernel, out_shape=jax.ShapeDtypeStruct((count, widt...  6.49 us
    ppermute x3, starting transfers between devices, body(): lax.ppermute(leaving, 'tp', [(i, (i + step) % tp_size) for i in range(tp_...  4.14 us
    reshape x1, local copies, waits for them, and re-layouts, body(): routed_result.reshape(ep_size, padded, model_width)[:, :capacity]  4.11 us
  transfers between devices with their start and end apart: 4, of which 3 were waited for; matrix products, arithmetic and copies ran while one was open for 1% of the time, Pallas kernels for 3%

profile of v3, /device:TPU:1, one launch (start us, length us, event | category | flops | bytes accessed | tf_op | source)
XLA Modules:
  0.0 197.7 jit_solution(18187907853028383280)
XLA Ops:
  0.6 0.0 copy-start
  0.7 1.6 fusion.3
  2.3 0.0 copy-start.3
  2.3 0.0 copy-start.7
  2.3 0.0 copy-start.9
  2.3 0.0 copy-start.6
  2.3 2.4 %fusion.12 = bf16[384,256]{1,0:T(8,128)(2,1)S(1)} fusion(bf16[2048,128]{1,0:T(8,128)(2,1)} %param.26, bf16[2048,128]{1,0:T(8,128)(2,1)} %param.23, bf16[2048,128]{1,0:T(8,128)(2,1)} %param.22, bf16[256,2048]{1,0:T(8,128)(2,1)} %param.20, f32[2048]{0:T(1024)} %param.21, f32[256]{0:T(256)S(1)} %add_rsqrt_fusion), kind=kOutput, calls=%fused_computation.20 | convolution fusion | flops 409567232 | bytes 2827264 | tf_op jit(solution)/shard_map/dot_general | solution.py:542
  4.8 0.0 copy-done.3
  4.8 0.2 fusion.16
  5.0 0.0 copy-done.7
  5.0 0.1 copy.40
  5.1 0.1 eq.42
  5.2 0.3 fusion.15
  5.5 0.1 convert_element_type.67
  5.7 0.0 copy-start.4
  5.7 0.0 copy-start.10
  5.7 0.0 copy-start.11
  5.7 0.0 copy-start.12
  5.7 0.1 copy.41
  5.8 0.1 fusion.25
  5.9 0.7 fusion.40
  6.6 0.0 copy-done.9
  6.6 0.7 copy.42.gain_ref
  7.3 0.0 copy-done.6
  7.3 0.2 fusion.18.rows_ref
  7.5 0.0 copy-start.1
  7.5 2.1 %convolution_convert_fusion.leaving_ref = bf16[512,2048]{1,0:T(8,128)(2,1)} fusion(pred[512,128]{1,0:T(8,128)(4,1)S(1)} %fusion.25, bf16[128,2048]{1,0:T(8,128)(2,1)S(1)} %fusion.18.rows_ref), kind=kOutput, calls=%fused_computation | convolution fusion | flops 269484032 | bytes 2686976 | tf_op jit(solution)/shard_map/dot_general | solution.py:564
  9.6 0.0 copy-done.4
  9.6 0.0 copy-done.10
  9.6 0.0 copy-done.11
  9.6 0.0 copy-done.12
  9.6 0.0 copy-start.13
  9.6 0.5 convolution_convert_fusion.2
  10.1 0.0 copy-done.1
  10.1 0.7 pad_maximum_fusion.block_ref
  10.8 0.0 copy-done.13
  10.8 0.6 broadcast_in_dim.10
  11.4 132.2 %attend.1 = (bf16[4,2048,128]{2,1,0:T(8,128)(2,1)}, bf16[4,2048,128]{2,1,0:T(8,128)(2,1)}, bf16[4,128,2048]{2,1,0:T(8,128)(2,1)}, bf16[512,2048]{1,0:T(8,128)(2,...) custom-call(bf16[2048,256]{1,0:T(8,128)(2,1)} %bitcast.36, bf16[2048,256]{1,0:T(8,128)(2,1)} %bitcast.37, ...), custom_call_target="tpu_custom_call" | custom-call | bytes 300000000 | tf_op jit(solution)/shard_map/attend/pallas_call | solution.py:469
  143.6 4.1 %reshape.58 = bf16[64,80,128]{2,1,0:T(8,128)(2,1)} reshape(bf16[64,5,2048]{2,1,0:T(8,128)(2,1)} %bitcast.35) | data formatting | bytes 2621440 | tf_op jit(solution)/shard_map/reshape | solution.py:571
  147.7 0.0 copy-start.5
  147.7 12.2 %all-to-all-start = ((bf16[64,80,128]{2,1,0:T(8,128)(2,1)}), bf16[64,80,128]{2,1,0:T(8,128)(2,1)}, u32[]{:S(2)}, u32[]{:S(2)}) async-start(bf16[64,80,128]{2,1,0:T(8,128)(2,1)} %reshape.58), calls=%async_computation | async-start | bytes 2621440 | tf_op jit(solution)/shard_map/all_to_all | solution.py:574
  160.0 0.0 copy-start.8
  160.0 0.0 copy-done
  160.0 0.0 copy-done.5
  160.0 0.4 convolution_convert_fusion.1
  160.5 0.1 dynamic-slice_bitcast_fusion.2
  160.6 3.0 %collective-permute-start.2 = (bf16[64,2048]{1,0:T(8,128)(2,1)S(1)}, bf16[64,2048]{1,0:T(8,128)(2,1)S(1)}, u32[]{:S(2)}, u32[]{:S(2)}) collective-permute-start(bf16[64,2048]{1,0:T(8,128)(2,1)S(1)} %get-tuple-element.25), channel_id=1, source_target_pairs={{0,3},{1,0},{2,1},{3,2},{4,7},{5,4},{6,5},{7,6},{8,11},{9,8},{10,9... | collective-permute-start | bytes 786440 | tf_op jit(solution)/shard_map/ppermute | solution.py:582
  163.6 0.4 collective-permute-start.1
  164.0 0.7 collective-permute-start
  164.7 0.0 copy-done.8
  164.7 6.5 %shared.1 = f32[128,2048]{1,0:T(8,128)} custom-call(bf16[128,2048]{1,0:T(8,128)(2,1)} %copy-done.1, bf16[4,2048,128]{2,1,0:T(8,128)(2,1)} %get-tuple-element.18.gate_ref, bf16[4,2048,128]{2,1,0:T(8,128)(2,1)} %get-tuple-element.19.up_ref, bf16[4,128,2048]{2,1,0:T(8,128)(2,1)} %get-tuple-element.20.down_ref), custom_call_target="tpu_custom_call" | custom-call | flops 805306368 | bytes 6291456 | tf_op jit(solution)/shard_map/shared/pallas_call | solution.py:107
  171.2 0.1 iota_compare_fusion.1
  171.3 2.9 %collective-permute-done.2 = bf16[64,2048]{1,0:T(8,128)(2,1)S(1)} collective-permute-done((bf16[64,2048]{1,0:T(8,128)(2,1)S(1)}, bf16[64,2048]{1,0:T(8,128)(2,1)S(1)}, u32[]{:S(2)}, u32[]{:S(2)}) %collective-permute-start.2) | collective-permute-done | bytes 262176 | tf_op jit(solution)/shard_map/ppermute | solution.py:582
  174.2 0.0 collective-permute-done.1
  174.2 4.8 %collective-permute-done = bf16[64,2048]{1,0:T(8,128)(2,1)} collective-permute-done((bf16[64,2048]{1,0:T(8,128)(2,1)S(1)}, bf16[64,2048]{1,0:T(8,128)(2,1)}, u32[]{:S(2)}, u32[]{:S(2)}) %collective-permute-start) | collective-permute-done | bytes 262176 | tf_op jit(solution)/shard_map/ppermute | solution.py:582
  179.0 1.8 fusion.24
  180.8 0.0 copy-start.2
  180.8 12.7 %all-to-all-done = bf16[64,80,128]{2,1,0:T(8,128)(2,1)} async-done(((bf16[64,80,128]{2,1,0:T(8,128)(2,1)}), bf16[64,80,128]{2,1,0:T(8,128)(2,1)}, u32[]{:S(2)}, u32[]{:S(2)}) %all-to-all-start) | async-done | bytes 1310752 | tf_op jit(solution)/shard_map/all_to_all | solution.py:574
  193.5 2.4 %reshape.60 = bf16[320,2048]{1,0:T(8,128)(2,1)S(1)} reshape(bf16[64,80,128]{2,1,0:T(8,128)(2,1)} %all-to-all-done) | data formatting | bytes 2621440 | tf_op jit(solution)/shard_map/reshape | solution.py:587
  195.9 0.5 convolution_multiply_fusion.1
  196.4 0.0 copy-done.2
  196.4 1.3 fusion.2
  (8 shorter events, 0.1 us)
Async XLA Ops:
  0.6 159.4 %copy-start = (bf16[256,2048]{1,0:T(8,128)(2,1)S(1)}, bf16[256,2048]{1,0:T(8,128)(2,1)}, u32[]{:S(2)}) copy-start(bf16[256,2048]{1,0:T(8,128)(2,1)} %param.29) | copy-start | bytes 3145732
  2.3 2.5 %copy-start.3 = (bf16[128,2048]{1,0:T(8,128)(2,1)S(1)}, bf16[128,2048]{1,0:T(8,128)(2,1)}, u32[]{:S(2)}) copy-start(bf16[128,2048]{1,0:T(8,128)(2,1)} %param.30) | copy-start | bytes 1572868
  2.3 2.7 %copy-start.7 = (s32[128,2]{0,1:T(2,128)S(1)}, s32[128,2]{0,1:T(2,128)}, u32[]{:S(2)}) copy-start(s32[128,2]{0,1:T(2,128)} %param.32) | copy-start | bytes 3076
  2.3 4.3 %copy-start.9 = (f32[128]{0:T(128)S(1)}, f32[128]{0:T(128)}, u32[]{:S(2)}) copy-start(f32[128]{0:T(128)} %param.28) | copy-start | bytes 1540
  2.3 5.0 %copy-start.6 = (f32[2048]{0:T(1024)S(1)}, f32[2048]{0:T(1024)}, u32[]{:S(2)}) copy-start(f32[2048]{0:T(1024)} %param.31) | copy-start | bytes 24580
  5.7 3.9 %copy-start.4 = (bf16[256,2048]{1,0:T(8,128)(2,1)S(1)}, bf16[256,2048]{1,0:T(8,128)(2,1)}, u32[]{:S(2)}) copy-start(bf16[256,2048]{1,0:T(8,128)(2,1)} %param.20) | copy-start | bytes 3145732
  5.7 3.9 %copy-start.10 = (bf16[2048,64]{0,1:T(8,128)(2,1)S(1)}, bf16[2048,64]{0,1:T(8,128)(2,1)}, u32[]{:S(2)}) copy-start(bf16[2048,64]{0,1:T(8,128)(2,1)} %param.25) | copy-start | bytes 786436
  5.7 3.9 %copy-start.11 = (bf16[2048,64]{0,1:T(8,128)(2,1)S(1)}, bf16[2048,64]{0,1:T(8,128)(2,1)}, u32[]{:S(2)}) copy-start(bf16[2048,64]{0,1:T(8,128)(2,1)} %param.24) | copy-start | bytes 786436
  5.7 3.8 %copy-start.12 = (f32[2048]{0:T(1024)S(1)}, f32[2048]{0:T(1024)}, u32[]{:S(2)}) copy-start(f32[2048]{0:T(1024)} %param.21) | copy-start | bytes 24580
  7.5 2.6 %copy-start.1 = (bf16[128,2048]{1,0:T(8,128)(2,1)}, bf16[128,2048]{1,0:T(8,128)(2,1)S(1)}, u32[]{:S(2)}) copy-start(bf16[128,2048]{1,0:T(8,128)(2,1)S(1)} %fusion.18.rows_ref) | copy-start | bytes 1572868
  9.6 1.2 copy-start.13
  147.7 12.3 %copy-start.5 = (bf16[256,256]{1,0:T(8,128)(2,1)S(1)}, bf16[256,256]{1,0:T(8,128)(2,1)}, u32[]{:S(2)}) copy-start(bf16[256,256]{1,0:T(8,128)(2,1)} %get-tuple-element.16) | copy-start | bytes 393220
  147.7 45.8 %all-to-all-start = ((bf16[64,80,128]{2,1,0:T(8,128)(2,1)}), bf16[64,80,128]{2,1,0:T(8,128)(2,1)}, u32[]{:S(2)}, u32[]{:S(2)}) async-start(bf16[64,80,128]{2,1,0:T(8,128)(2,1)} %reshape.58), calls=%async_computation | async-start | bytes 2621440 | tf_op jit(solution)/shard_map/all_to_all | solution.py:574
  160.0 4.7 %copy-start.8 = (f32[128,2]{0,1:T(2,128)S(1)}, f32[128,2]{0,1:T(2,128)}, u32[]{:S(2)}) copy-start(f32[128,2]{0,1:T(2,128)} %param.33) | copy-start | bytes 3076
  160.6 13.6 %collective-permute-start.2 = (bf16[64,2048]{1,0:T(8,128)(2,1)S(1)}, bf16[64,2048]{1,0:T(8,128)(2,1)S(1)}, u32[]{:S(2)}, u32[]{:S(2)}) collective-permute-start(bf16[64,2048]{1,0:T(8,128)(2,1)S(1)} %get-tuple-element.25), channel_id=1, source_target_pairs={{0,3},{1,0},{2,1},{3,2},{4,7},{5,4},{6,5},{7,6},{8,11},{9,8},{10,9... | collective-permute-start | bytes 786440 | tf_op jit(solution)/shard_map/ppermute | solution.py:582
  163.6 10.6 %collective-permute-start.1 = (bf16[64,2048]{1,0:T(8,128)(2,1)S(1)}, bf16[64,2048]{1,0:T(8,128)(2,1)S(1)}, u32[]{:S(2)}, u32[]{:S(2)}) collective-permute-start(bf16[64,2048]{1,0:T(8,128)(2,1)S(1)} %get-tuple-element.26), channel_id=1, source_target_pairs={{0,2},{1,3},{2,0},{3,1},{4,6},{5,7},{6,4},{7,5},{8,10},{9,11},{10,... | collective-permute-start | bytes 786440 | tf_op jit(solution)/shard_map/ppermute | solution.py:582
  164.0 15.0 %collective-permute-start = (bf16[64,2048]{1,0:T(8,128)(2,1)S(1)}, bf16[64,2048]{1,0:T(8,128)(2,1)}, u32[]{:S(2)}, u32[]{:S(2)}) collective-permute-start(bf16[64,2048]{1,0:T(8,128)(2,1)S(1)} %get-tuple-element.24), channel_id=1, source_target_pairs={{0,1},{1,2},{2,3},{3,0},{4,5},{5,6},{6,7},{7,4},{8,9},{9,10},{10,1... | collective-permute-start | bytes 786440 | tf_op jit(solution)/shard_map/ppermute | solution.py:582
  180.8 15.6 %copy-start.2 = (f32[128,2048]{1,0:T(8,128)S(1)}, f32[128,2048]{1,0:T(8,128)}, u32[]{:S(2)}) copy-start(f32[128,2048]{1,0:T(8,128)} %shared.1) | copy-start | bytes 3145732

commit v4 on v3

--- a/solution.py
+++ b/solution.py
@@ -71,12 +71,13 @@
         lax.fori_loop(0, steps, step, 0)
         block(which, steps, True, full * rows + which * half)
         mixed = [weighted[which, m] / totals[which, m] for m in range(2)]
-        combined = mixed[0] - lam_ref[...] * mixed[1]
+        lane = lax.broadcasted_iota(jnp.int32, (1, 2 * half), 1)
+        combined = mixed[0] - jnp.where(lane < half, lam_ref[0], lam_ref[1]) * mixed[1]
         factor = lax.rsqrt(jnp.mean(combined * combined, axis=0, keepdims=True) + EPS)
-        normed = combined * factor * gain_ref[...]
+        normed = combined * factor
         for head in range(2):
             part = normed[:, head * half : (head + 1) * half]
-            results[which][0:half, head * 128 : (head + 1) * 128] = part.T.astype(jnp.bfloat16)
+            results[which][0:half, head * 128 : (head + 1) * 128] = (part.T * gain_ref[...]).astype(jnp.bfloat16)
 
 
 def expert_kernel(rows_ref, gate_ref, up_ref, down_ref, out_ref, total):
@@ -276,18 +277,33 @@
     shared_gate_ref,
     shared_up_ref,
     shared_down_ref,
-    leaving_ref,
-    low_ref,
-    high_ref,
-    block_ref,
+    mixer_ref,
+    query_one_ref,
+    query_two_ref,
+    value_ref,
+    key_one_ref,
+    key_two_ref,
+    expert_ref,
+    slot_ref,
+    mixer_gain_ref,
+    expert_gain_ref,
     lam_ref,
     gain_ref,
     shared_gate_out,
     shared_up_out,
     shared_down_out,
+    leaving_ref,
     landed_ref,
     routed_ref,
     out_ref,
+    mixer_rows,
+    projections,
+    key_rows,
+    expert_rows,
+    low_ref,
+    high_ref,
+    block_ref,
+    load_sem,
     gate_all,
     up_all,
     down_all,
@@ -336,15 +352,58 @@
     targets = (shared_gate_out, shared_up_out, shared_down_out)
     tp_peers = (ring.sides[1], opposite, ring.sides[0])
     spread = Spread(sources, targets, x, core, tp_peers, across, other, sems[5:])
+    loads = [(mixer_ref, mixer_rows), (expert_ref, expert_rows)]
+    loads += [(w, projections.at[i]) for i, w in enumerate((query_one_ref, query_two_ref, value_ref))]
+    loads += [(w, key_rows.at[pl.ds(i * HEAD, HEAD)]) for i, w in enumerate((key_one_ref, key_two_ref))]
+    loads = [pltpu.make_async_copy(source, target, load_sem.at[i]) for i, (source, target) in enumerate(loads)]
+    for copy in loads:
+        copy.start()
     greet(ring.sides + (opposite,), count)
+    spread.start()
+    ring.start()
+    for copy in loads:
+        copy.wait()
+
+    half = mixer_rows.shape[0] // 2
+    mixer_rows[...] = normalize(mixer_rows[...], mixer_gain_ref[...])
+    normed = mixer_rows[...]
+
+    def project(i):
+        product = jnp.dot(normed, projections[i], preferred_element_type=jnp.float32)
+        return product.astype(jnp.bfloat16)
+
+    def turned(product, scale):
+        return (product.astype(jnp.float32).T * scale).astype(jnp.bfloat16)
+
+    keys = lax.dot_general(normed, key_rows[...], (((1,), (1,)), ((), ())), preferred_element_type=jnp.float32)
+    block_ref[0 : 2 * half] = keys.astype(jnp.bfloat16)
+    value_turned = turned(project(2), 1.0)
+    for part in range(2):
+        block_ref[(2 + part) * half : (3 + part) * half] = value_turned[:, part * half : (part + 1) * half]
+    for m in range(2):
+        query_turned = turned(project(m), HEAD ** (-0.5))
+        low_ref[m * 2 * HEAD : (m + 1) * 2 * HEAD] = query_turned[:, 0:half]
+        high_ref[m * 2 * HEAD : (m + 1) * 2 * HEAD] = query_turned[:, half : 2 * half]
+
+    expert_rows[...] = normalize(expert_rows[...], expert_gain_ref[...])
+    slot = lax.broadcasted_iota(jnp.int32, (landed.shape[0], expert_rows.shape[0]), 0)
+    match = slot == slot_ref[0:1, :]
+    for k in range(1, slot_ref.shape[0]):
+        match = jnp.logical_or(match, slot == slot_ref[k : k + 1, :])
+    select = jnp.where(match, 1.0, 0.0).astype(jnp.bfloat16)
+    width = 512
+    for i in range(expert_rows.shape[1] // width):
+        span = slice(i * width, (i + 1) * width)
+        chosen = jnp.dot(select, expert_rows[:, span], preferred_element_type=jnp.float32)
+        landed[:, span] = chosen.astype(jnp.bfloat16)
+    leave = pltpu.make_async_copy(landed, leaving_ref, load_sem.at[7])
+    leave.start()
 
     own_view = kv_ref.at[chip, core]
     along_x = [send(block_ref, own_view, send_x.at[k], recv_x.at[k], across[k]) for k in range(3)]
     own_block = pltpu.make_async_copy(block_ref, own_view, block_sem)
     own_block.start()
     asked = send(high_ref, swapped, send_query, recv_query, mirror)
-    spread.start()
-    ring.start()
     own_block.wait()
     for copy in along_x:
         copy.wait_recv()
@@ -401,6 +460,7 @@
         row_copy(k).wait()
         return carry
 
+    leave.wait()
     lax.fori_loop(1, count, start_rows, 0)
     own_rows = pltpu.make_async_copy(rows_of(leaving_ref, place), rows_of(landed_ref, place), send_rows.at[0])
     own_rows.start()
@@ -456,24 +516,37 @@
     ring.finish_sends()
 
 
-def attend(weights, leaving, low, high, block, lambdas, head_gain):
+def attend(weights, mixer, projections, expert, slots, slot_rows, mixer_gain, expert_gain, lambdas, head_gain):
     size = lax.axis_size("tp")
     count = lax.axis_size("ep")
-    half = block.shape[0] // 4
+    half = mixer.shape[0] // 2
+    width = mixer.shape[1]
     value_dim = head_gain.shape[0]
-    lam = jnp.repeat(lambdas, half).reshape(1, 2 * half)
     vmem = pl.BlockSpec(memory_space=pltpu.VMEM)
     hbm = pl.BlockSpec(memory_space=pltpu.HBM)
     dma = pltpu.SemaphoreType.DMA
     steps = count // (4 * NX)
+    block = jax.ShapeDtypeStruct((4 * half, value_dim), jnp.bfloat16)
+    high = jax.ShapeDtypeStruct((4 * HEAD, half), jnp.bfloat16)
+    leaving = jax.ShapeDtypeStruct((slot_rows, width), jnp.bfloat16)
     return pl.pallas_call(
         attend_kernel,
         out_shape=[jax.ShapeDtypeStruct((size,) + w.shape, w.dtype) for w in weights[3:]]
-        + [jax.ShapeDtypeStruct(leaving.shape, leaving.dtype)] * 2
+        + [leaving] * 3
         + [jax.ShapeDtypeStruct((2 * half, 2 * value_dim), jnp.bfloat16)],
-        in_specs=[hbm] * 7 + [vmem] * 5,
-        out_specs=[hbm] * 4 + [vmem] * 2,
-        scratch_shapes=[pltpu.VMEM((size,) + w.shape, w.dtype) for w in weights[:3]]
+        in_specs=[hbm] * 13 + [vmem] * 3 + [pl.BlockSpec(memory_space=pltpu.SMEM), vmem],
+        out_specs=[hbm] * 5 + [vmem] * 2,
+        scratch_shapes=[
+            pltpu.VMEM(mixer.shape, mixer.dtype),
+            pltpu.VMEM((3,) + projections[0].shape, jnp.bfloat16),
+            pltpu.VMEM((2 * HEAD, width), jnp.bfloat16),
+            pltpu.VMEM(expert.shape, expert.dtype),
+            pltpu.VMEM(high.shape, high.dtype),
+            pltpu.VMEM(high.shape, high.dtype),
+            pltpu.VMEM(block.shape, block.dtype),
+            dma((8,)),
+        ]
+        + [pltpu.VMEM((size,) + w.shape, w.dtype) for w in weights[:3]]
         + [
             pltpu.VMEM(leaving.shape, leaving.dtype),
             pltpu.VMEM(leaving.shape, jnp.float32),
@@ -504,7 +577,17 @@
         cost_estimate=pl.CostEstimate(flops=0, bytes_accessed=300_000_000, transcendentals=0),
         compiler_params=pltpu.CompilerParams(collective_id=0, has_side_effects=True, vmem_limit_bytes=60 * 1024 * 1024),
         name="attend",
-    )(*weights, leaving, low, high, block, lam, head_gain.reshape(value_dim, 1))
+    )(
+        *weights,
+        mixer,
+        *projections,
+        expert,
+        slots,
+        mixer_gain.reshape(1, width),
+        expert_gain.reshape(1, width),
+        lambdas,
+        head_gain.reshape(1, value_dim),
+    )
 
 
 def body(
@@ -536,17 +619,6 @@
     half_rows = mixer_rows // 2
     token_rows = expert_input.shape[0]
 
-    normed = normalize(mixer_input, mixer_gain)
-    query_cols = query_one.shape[1]
-    turned_weight = jnp.concatenate([query_one, query_two, value_weight], axis=1)
-    turned = lax.dot_general(turned_weight, normed, (((0,), (1,)), ((), ())), preferred_element_type=jnp.float32)
-    keys = jnp.dot(normed, jnp.concatenate([key_one, key_two], axis=1), preferred_element_type=jnp.float32)
-    keys = keys.astype(jnp.bfloat16)
-    queries = (turned[: 2 * query_cols].astype(jnp.bfloat16) * HEAD ** (-0.5)).astype(jnp.bfloat16)
-    values = turned[2 * query_cols :].astype(jnp.bfloat16)
-    key_values = jnp.concatenate([keys, values[:, :half_rows], values[:, half_rows:]], axis=0)
-
-    normed_experts = normalize(expert_input, expert_gain)
     expert_count = expert_gate.shape[0] * ep_size
     top_count = routes.shape[1]
     capacity = max(2, 5 * token_rows * top_count // (4 * expert_count))
@@ -559,18 +631,24 @@
     slot_ids = (flat_routes * capacity + slot_place).reshape(token_rows, top_count)
     padded = -(-capacity // 8) * 8
     leaving_ids = (flat_routes * padded + slot_place).reshape(token_rows, top_count)
-    slot_match = jnp.arange(expert_count * padded, dtype=jnp.int32)[:, None, None] == leaving_ids[None, :, :]
-    select = jnp.any(slot_match, axis=2).astype(jnp.bfloat16)
-    outgoing = jnp.dot(select, normed_experts, preferred_element_type=jnp.float32).astype(jnp.bfloat16)
-
     weights = (expert_gate[0], expert_up[0], expert_down[0], shared_gate, shared_up, shared_down)
-    *shared_weights, _, routed_result, head_rows = attend(
-        weights, outgoing, queries[:, :half_rows], queries[:, half_rows:], key_values, lambdas, head_gain
+    *shared_weights, _, _, routed_result, head_rows = attend(
+        weights,
+        mixer_input,
+        (query_one, query_two, value_weight, key_one.T, key_two.T),
+        expert_input,
+        leaving_ids.T,
+        expert_count * padded,
+        mixer_gain,
+        expert_gain,
+        lambdas,
+        head_gain,
     )
     lines = slot_count // ep_size * model_width // 128
     routed_result = routed_result.reshape(ep_size, padded, model_width)[:, :capacity].reshape(ep_size, lines, 128)
 
-    normed_again, head_rows, routed_result = lax.optimization_barrier((normed_experts, head_rows, routed_result))
+    expert_rows, head_rows, routed_result = lax.optimization_barrier((expert_input, head_rows, routed_result))
+    normed_again = normalize(expert_rows, expert_gain)
     returned = lax.all_to_all(routed_result, "ep", split_axis=0, concat_axis=0, tiled=True)
     shared_result = swiglu_groups(normed_again, *shared_weights, jnp.float32, "shared")
     partial = jnp.dot(head_rows, output_weight, preferred_element_type=jnp.float32).astype(jnp.bfloat16)

time: 198 us -> 193 us (0.975)
  matrix products: 7.5 us -> 2.5 us
    dot_general x3 -> x0, matrix products: 4.97 us -> none  [the longest x1 2.42 us: body(): lax.dot_general(turned_weight, normed, (((0,), (1,)), ((), ())), preferre...]
  transfers between devices with their start and end apart: 4 -> 4, of which waited for: 3 -> 3; matrix products, arithmetic and copies ran while one was open for 1% -> 2% of each run, Pallas kernels for 3% -> 3%
where the time goes in v4:
time: 193 us; the launch traced here: 192 us
  Pallas kernels  139 us (72%)
  waiting for transfers between devices  19.8 us (10%)
  starting transfers between devices  17.8 us (9%)
  local copies, waits for them, and re-layouts  8.5 us (4%)
  other arithmetic  4.29 us (2%)
  matrix products  2.5 us (1%)
    pallas_call x1, Pallas kernels, attend(): pl.pallas_call(attend_kernel, out_shape=[jax.ShapeDtypeStruct((size,) + w...  132 us
    all_to_all x1, starting transfers between devices, body(): lax.all_to_all(routed_result, 'ep', split_axis=0, concat_axis=0, tiled=True)  14.1 us
    all_to_all x1, waiting for transfers between devices, body(): lax.all_to_all(routed_result, 'ep', split_axis=0, concat_axis=0, tiled=True)  13.1 us
    ppermute x3, waiting for transfers between devices, body(): lax.ppermute(leaving, 'tp', [(i, (i + step) % tp_size) for i in range(tp_...  6.67 us
    pallas_call x1, Pallas kernels, swiglu_groups(): pl.pallas_call(expert_kernel, out_shape=jax.ShapeDtypeStruct((count, widt...  6.48 us
    reshape x1, local copies, waits for them, and re-layouts, body(): routed_result.reshape(ep_size, padded, model_width)[:, :capacity]  4.12 us
  transfers between devices with their start and end apart: 4, of which 3 were waited for; matrix products, arithmetic and copies ran while one was open for 2% of the time, Pallas kernels for 3%

profile of v4, /device:TPU:1, one launch (start us, length us, event | category | flops | bytes accessed | tf_op | source)
XLA Modules:
  0.0 192.4 jit_solution(2518179817986572973)
XLA Ops:
  0.6 0.0 copy-start
  0.7 0.9 copy.28
  1.5 0.1 eq.28
  1.7 0.3 fusion.3
  2.0 0.1 convert_element_type.49
  2.1 0.1 copy.29
  2.2 1.3 multiply_add_fusion
  3.4 132.2 %attend.1 = (bf16[4,2048,128]{2,1,0:T(8,128)(2,1)}, bf16[4,2048,128]{2,1,0:T(8,128)(2,1)}, bf16[4,128,2048]{2,1,0:T(8,128)(2,1)}, bf16[512,2048]{1,0:T(8,128)(2,...) custom-call(bf16[2048,256]{1,0:T(8,128)(2,1)} %bitcast.39, ...), custom_call_target="tpu_custom_call" | custom-call | bytes 300000000 | tf_op jit(solution)/shard_map/attend/pallas_call | solution.py:532
  135.7 4.1 %reshape.52 = bf16[64,80,128]{2,1,0:T(8,128)(2,1)} reshape(bf16[64,5,2048]{2,1,0:T(8,128)(2,1)} %bitcast.38) | data formatting | bytes 2621440 | tf_op jit(solution)/shard_map/reshape | solution.py:648
  139.8 0.0 copy-start.3
  139.8 14.1 %all-to-all-start = ((bf16[64,80,128]{2,1,0:T(8,128)(2,1)}), bf16[64,80,128]{2,1,0:T(8,128)(2,1)}, u32[]{:S(2)}, u32[]{:S(2)}) async-start(bf16[64,80,128]{2,1,0:T(8,128)(2,1)} %reshape.52), calls=%async_computation | async-start | bytes 2621440 | tf_op jit(solution)/shard_map/all_to_all | solution.py:652
  153.9 0.0 copy-done
  153.9 0.0 copy-done.3
  154.0 0.4 convolution_convert_fusion
  154.4 0.0 copy-start.1
  154.4 0.0 copy-start.5
  154.4 0.0 copy-start.4
  154.4 0.1 dynamic-slice_bitcast_fusion.2
  154.5 2.8 %collective-permute-start.2 = (bf16[64,2048]{1,0:T(8,128)(2,1)S(1)}, bf16[64,2048]{1,0:T(8,128)(2,1)S(1)}, u32[]{:S(2)}, u32[]{:S(2)}) collective-permute-start(bf16[64,2048]{1,0:T(8,128)(2,1)S(1)} %get-tuple-element.25), channel_id=1, source_target_pairs={{0,3},{1,0},{2,1},{3,2},{4,7},{5,4},{6,5},{7,6},{8,11},{9,8},{10,9... | collective-permute-start | bytes 786440 | tf_op jit(solution)/shard_map/ppermute | solution.py:660
  157.3 0.2 collective-permute-start.1
  157.5 0.7 collective-permute-start
  158.2 0.0 copy-done.1
  158.2 0.2 fusion.4
  158.4 0.0 copy-done.5
  158.4 0.0 copy-done.4
  158.4 1.0 fusion.6.rows_ref
  159.4 6.5 %shared.1 = f32[128,2048]{1,0:T(8,128)} custom-call(bf16[128,2048]{1,0:T(8,128)(2,1)} %fusion.6.rows_ref, bf16[4,2048,128]{2,1,0:T(8,128)(2,1)} %get-tuple-element.18.gate_ref, bf16[4,2048,128]{2,1,0:T(8,128)(2,1)} %get-tuple-element.19.up_ref, bf16[4,128,2048]{2,1,0:T(8,128)(2,1)} %get-tuple-element.20.down_ref), custom_call_target="tpu_custom_call" | custom-call | flops 805306368 | bytes 6291456 | tf_op jit(solution)/shard_map/shared/pallas_call | solution.py:108
  165.9 0.1 iota_compare_fusion
  165.9 2.0 %collective-permute-done.2 = bf16[64,2048]{1,0:T(8,128)(2,1)S(1)} collective-permute-done((bf16[64,2048]{1,0:T(8,128)(2,1)S(1)}, bf16[64,2048]{1,0:T(8,128)(2,1)S(1)}, u32[]{:S(2)}, u32[]{:S(2)}) %collective-permute-start.2) | collective-permute-done | bytes 262176 | tf_op jit(solution)/shard_map/ppermute | solution.py:660
  167.9 0.0 collective-permute-done.1
  167.9 4.7 %collective-permute-done = bf16[64,2048]{1,0:T(8,128)(2,1)} collective-permute-done((bf16[64,2048]{1,0:T(8,128)(2,1)S(1)}, bf16[64,2048]{1,0:T(8,128)(2,1)}, u32[]{:S(2)}, u32[]{:S(2)}) %collective-permute-start) | collective-permute-done | bytes 262176 | tf_op jit(solution)/shard_map/ppermute | solution.py:660
  172.6 1.8 fusion.9
  174.4 13.1 %all-to-all-done = bf16[64,80,128]{2,1,0:T(8,128)(2,1)} async-done(((bf16[64,80,128]{2,1,0:T(8,128)(2,1)}), bf16[64,80,128]{2,1,0:T(8,128)(2,1)}, u32[]{:S(2)}, u32[]{:S(2)}) %all-to-all-start) | async-done | bytes 1310752 | tf_op jit(solution)/shard_map/all_to_all | solution.py:652
  187.5 2.4 %reshape.54 = bf16[320,2048]{1,0:T(8,128)(2,1)S(1)} reshape(bf16[64,80,128]{2,1,0:T(8,128)(2,1)} %all-to-all-done) | data formatting | bytes 2621440 | tf_op jit(solution)/shard_map/reshape | solution.py:665
  189.9 0.0 copy-start.2
  189.9 0.5 convolution_multiply_fusion.1
  190.4 0.7 copy-done.2
  191.1 1.3 fusion.2
  (4 shorter events, 0.0 us)
Async XLA Ops:
  0.6 153.3 %copy-start = (bf16[256,2048]{1,0:T(8,128)(2,1)S(1)}, bf16[256,2048]{1,0:T(8,128)(2,1)}, u32[]{:S(2)}) copy-start(bf16[256,2048]{1,0:T(8,128)(2,1)} %param.29) | copy-start | bytes 3145732
  139.8 14.2 %copy-start.3 = (bf16[256,256]{1,0:T(8,128)(2,1)S(1)}, bf16[256,256]{1,0:T(8,128)(2,1)}, u32[]{:S(2)}) copy-start(bf16[256,256]{1,0:T(8,128)(2,1)} %get-tuple-element.16) | copy-start | bytes 393220
  139.8 47.7 %all-to-all-start = ((bf16[64,80,128]{2,1,0:T(8,128)(2,1)}), bf16[64,80,128]{2,1,0:T(8,128)(2,1)}, u32[]{:S(2)}, u32[]{:S(2)}) async-start(bf16[64,80,128]{2,1,0:T(8,128)(2,1)} %reshape.52), calls=%async_computation | async-start | bytes 2621440 | tf_op jit(solution)/shard_map/all_to_all | solution.py:652
  154.4 3.8 %copy-start.1 = (bf16[128,2048]{1,0:T(8,128)(2,1)S(1)}, bf16[128,2048]{1,0:T(8,128)(2,1)}, u32[]{:S(2)}) copy-start(bf16[128,2048]{1,0:T(8,128)(2,1)} %expert_ref.1) | copy-start | bytes 1572868
  154.4 4.0 %copy-start.5 = (f32[128,2]{0,1:T(2,128)S(1)}, f32[128,2]{0,1:T(2,128)}, u32[]{:S(2)}) copy-start(f32[128,2]{0,1:T(2,128)} %param.33) | copy-start | bytes 3076
  154.4 4.0 %copy-start.4 = (f32[2048]{0:T(1024)S(1)}, f32[2048]{0:T(1024)}, u32[]{:S(2)}) copy-start(f32[2048]{0:T(1024)} %param.31) | copy-start | bytes 24580
  154.5 13.4 %collective-permute-start.2 = (bf16[64,2048]{1,0:T(8,128)(2,1)S(1)}, bf16[64,2048]{1,0:T(8,128)(2,1)S(1)}, u32[]{:S(2)}, u32[]{:S(2)}) collective-permute-start(bf16[64,2048]{1,0:T(8,128)(2,1)S(1)} %get-tuple-element.25), channel_id=1, source_target_pairs={{0,3},{1,0},{2,1},{3,2},{4,7},{5,4},{6,5},{7,6},{8,11},{9,8},{10,9... | collective-permute-start | bytes 786440 | tf_op jit(solution)/shard_map/ppermute | solution.py:660
  157.3 10.6 %collective-permute-start.1 = (bf16[64,2048]{1,0:T(8,128)(2,1)S(1)}, bf16[64,2048]{1,0:T(8,128)(2,1)S(1)}, u32[]{:S(2)}, u32[]{:S(2)}) collective-permute-start(bf16[64,2048]{1,0:T(8,128)(2,1)S(1)} %get-tuple-element.26), channel_id=1, source_target_pairs={{0,2},{1,3},{2,0},{3,1},{4,6},{5,7},{6,4},{7,5},{8,10},{9,11},{10,... | collective-permute-start | bytes 786440 | tf_op jit(solution)/shard_map/ppermute | solution.py:660
  157.5 15.1 %collective-permute-start = (bf16[64,2048]{1,0:T(8,128)(2,1)S(1)}, bf16[64,2048]{1,0:T(8,128)(2,1)}, u32[]{:S(2)}, u32[]{:S(2)}) collective-permute-start(bf16[64,2048]{1,0:T(8,128)(2,1)S(1)} %get-tuple-element.24), channel_id=1, source_target_pairs={{0,1},{1,2},{2,3},{3,0},{4,5},{5,6},{6,7},{7,4},{8,9},{9,10},{10,1... | collective-permute-start | bytes 786440 | tf_op jit(solution)/shard_map/ppermute | solution.py:660
  189.9 1.2 copy-start.2

commit v5 on v4

--- a/solution.py
+++ b/solution.py
@@ -361,7 +361,7 @@
     greet(ring.sides + (opposite,), count)
     spread.start()
     ring.start()
-    for copy in loads:
+    for copy in loads[:1] + loads[2:]:
         copy.wait()
 
     half = mixer_rows.shape[0] // 2
@@ -385,6 +385,12 @@
         low_ref[m * 2 * HEAD : (m + 1) * 2 * HEAD] = query_turned[:, 0:half]
         high_ref[m * 2 * HEAD : (m + 1) * 2 * HEAD] = query_turned[:, half : 2 * half]
 
+    own_view = kv_ref.at[chip, core]
+    along_x = [send(block_ref, own_view, send_x.at[k], recv_x.at[k], across[k]) for k in range(3)]
+    own_block = pltpu.make_async_copy(block_ref, own_view, block_sem)
+    own_block.start()
+
+    loads[1].wait()
     expert_rows[...] = normalize(expert_rows[...], expert_gain_ref[...])
     slot = lax.broadcasted_iota(jnp.int32, (landed.shape[0], expert_rows.shape[0]), 0)
     match = slot == slot_ref[0:1, :]
@@ -399,10 +405,6 @@
     leave = pltpu.make_async_copy(landed, leaving_ref, load_sem.at[7])
     leave.start()
 
-    own_view = kv_ref.at[chip, core]
-    along_x = [send(block_ref, own_view, send_x.at[k], recv_x.at[k], across[k]) for k in range(3)]
-    own_block = pltpu.make_async_copy(block_ref, own_view, block_sem)
-    own_block.start()
     asked = send(high_ref, swapped, send_query, recv_query, mirror)
     own_block.wait()
     for copy in along_x:
@@ -453,7 +455,7 @@
         )
 
     def start_rows(k, carry):
-        row_copy(k).start()
+        row_copy(jnp.where(lax.rem(k, 2) == 1, lax.div(k + 1, 2), count - lax.div(k, 2))).start()
         return carry
 
     def wait_rows(k, carry):

time: 193 us -> 192 us (level)
  starting transfers between devices: 17.8 us -> 11.4 us
  Pallas kernels: 139 us -> 144 us
    all_to_all x1, starting transfers between devices: 14.1 us -> 7.76 us  [body(): lax.all_to_all(routed_result, 'ep', split_axis=0, concat_axis=0, tiled=True)]
    pallas_call x1, Pallas kernels: 132 us -> 137 us  [attend(): pl.pallas_call(attend_kernel, out_shape=[jax.ShapeDtypeStruct((size,) + w...]
where the time goes in v5:
time: 192 us; the launch traced here: 191 us
  Pallas kernels  144 us (75%)
  waiting for transfers between devices  19.8 us (10%)
  starting transfers between devices  11.4 us (6%)
  local copies, waits for them, and re-layouts  8.5 us (4%)
  other arithmetic  4.29 us (2%)
  matrix products  2.5 us (1%)
    pallas_call x1, Pallas kernels, attend(): pl.pallas_call(attend_kernel, out_shape=[jax.ShapeDtypeStruct((size,) + w...  137 us
    all_to_all x1, waiting for transfers between devices, body(): lax.all_to_all(routed_result, 'ep', split_axis=0, concat_axis=0, tiled=True)  13.4 us
    all_to_all x1, starting transfers between devices, body(): lax.all_to_all(routed_result, 'ep', split_axis=0, concat_axis=0, tiled=True)  7.76 us
    pallas_call x1, Pallas kernels, swiglu_groups(): pl.pallas_call(expert_kernel, out_shape=jax.ShapeDtypeStruct((count, widt...  6.48 us
    ppermute x3, waiting for transfers between devices, body(): lax.ppermute(leaving, 'tp', [(i, (i + step) % tp_size) for i in range(tp_...  6.45 us
    reshape x1, local copies, waits for them, and re-layouts, body(): routed_result.reshape(ep_size, padded, model_width)[:, :capacity]  4.12 us
  transfers between devices with their start and end apart: 4, of which 3 were waited for; matrix products, arithmetic and copies ran while one was open for 2% of the time, Pallas kernels for 3%

profile of v5, /device:TPU:1, one launch (start us, length us, event | category | flops | bytes accessed | tf_op | source)
XLA Modules:
  0.0 191.2 jit_solution(15863831277818487014)
XLA Ops:
  0.6 0.0 copy-start
  0.7 0.9 copy.28
  1.5 0.1 eq.28
  1.7 0.3 fusion.3
  2.0 0.1 convert_element_type.49
  2.1 0.1 copy.29
  2.2 1.3 multiply_add_fusion
  3.4 137.4 %attend.1 = (bf16[4,2048,128]{2,1,0:T(8,128)(2,1)}, bf16[4,2048,128]{2,1,0:T(8,128)(2,1)}, bf16[4,128,2048]{2,1,0:T(8,128)(2,1)}, bf16[512,2048]{1,0:T(8,128)(2,...) custom-call(bf16[2048,256]{1,0:T(8,128)(2,1)} %bitcast.39, ...), custom_call_target="tpu_custom_call" | custom-call | bytes 300000000 | tf_op jit(solution)/shard_map/attend/pallas_call | solution.py:534
  140.9 4.1 %reshape.52 = bf16[64,80,128]{2,1,0:T(8,128)(2,1)} reshape(bf16[64,5,2048]{2,1,0:T(8,128)(2,1)} %bitcast.38) | data formatting | bytes 2621440 | tf_op jit(solution)/shard_map/reshape | solution.py:650
  145.0 0.0 copy-start.3
  145.0 7.8 %all-to-all-start = ((bf16[64,80,128]{2,1,0:T(8,128)(2,1)}), bf16[64,80,128]{2,1,0:T(8,128)(2,1)}, u32[]{:S(2)}, u32[]{:S(2)}) async-start(bf16[64,80,128]{2,1,0:T(8,128)(2,1)} %reshape.52), calls=%async_computation | async-start | bytes 2621440 | tf_op jit(solution)/shard_map/all_to_all | solution.py:654
  152.8 0.0 copy-done
  152.8 0.0 copy-done.3
  152.8 0.4 convolution_convert_fusion
  153.3 0.0 copy-start.1
  153.3 0.0 copy-start.5
  153.3 0.0 copy-start.4
  153.3 0.1 dynamic-slice_bitcast_fusion.2
  153.4 2.9 %collective-permute-start.2 = (bf16[64,2048]{1,0:T(8,128)(2,1)S(1)}, bf16[64,2048]{1,0:T(8,128)(2,1)S(1)}, u32[]{:S(2)}, u32[]{:S(2)}) collective-permute-start(bf16[64,2048]{1,0:T(8,128)(2,1)S(1)} %get-tuple-element.25), channel_id=1, source_target_pairs={{0,3},{1,0},{2,1},{3,2},{4,7},{5,4},{6,5},{7,6},{8,11},{9,8},{10,9... | collective-permute-start | bytes 786440 | tf_op jit(solution)/shard_map/ppermute | solution.py:662
  156.3 0.0 collective-permute-start.1
  156.3 0.7 collective-permute-start
  157.0 0.0 copy-done.1
  157.0 0.2 fusion.4
  157.2 0.0 copy-done.5
  157.2 0.0 copy-done.4
  157.2 1.0 fusion.6.rows_ref
  158.2 6.5 %shared.1 = f32[128,2048]{1,0:T(8,128)} custom-call(bf16[128,2048]{1,0:T(8,128)(2,1)} %fusion.6.rows_ref, bf16[4,2048,128]{2,1,0:T(8,128)(2,1)} %get-tuple-element.18.gate_ref, bf16[4,2048,128]{2,1,0:T(8,128)(2,1)} %get-tuple-element.19.up_ref, bf16[4,128,2048]{2,1,0:T(8,128)(2,1)} %get-tuple-element.20.down_ref), custom_call_target="tpu_custom_call" | custom-call | flops 805306368 | bytes 6291456 | tf_op jit(solution)/shard_map/shared/pallas_call | solution.py:108
  164.7 0.1 iota_compare_fusion
  164.7 2.2 %collective-permute-done.2 = bf16[64,2048]{1,0:T(8,128)(2,1)S(1)} collective-permute-done((bf16[64,2048]{1,0:T(8,128)(2,1)S(1)}, bf16[64,2048]{1,0:T(8,128)(2,1)S(1)}, u32[]{:S(2)}, u32[]{:S(2)}) %collective-permute-start.2) | collective-permute-done | bytes 262176 | tf_op jit(solution)/shard_map/ppermute | solution.py:662
  166.9 0.0 collective-permute-done.1
  166.9 4.3 %collective-permute-done = bf16[64,2048]{1,0:T(8,128)(2,1)} collective-permute-done((bf16[64,2048]{1,0:T(8,128)(2,1)S(1)}, bf16[64,2048]{1,0:T(8,128)(2,1)}, u32[]{:S(2)}, u32[]{:S(2)}) %collective-permute-start) | collective-permute-done | bytes 262176 | tf_op jit(solution)/shard_map/ppermute | solution.py:662
  171.2 1.8 fusion.9
  173.0 13.4 %all-to-all-done = bf16[64,80,128]{2,1,0:T(8,128)(2,1)} async-done(((bf16[64,80,128]{2,1,0:T(8,128)(2,1)}), bf16[64,80,128]{2,1,0:T(8,128)(2,1)}, u32[]{:S(2)}, u32[]{:S(2)}) %all-to-all-start) | async-done | bytes 1310752 | tf_op jit(solution)/shard_map/all_to_all | solution.py:654
  186.3 2.4 %reshape.54 = bf16[320,2048]{1,0:T(8,128)(2,1)S(1)} reshape(bf16[64,80,128]{2,1,0:T(8,128)(2,1)} %all-to-all-done) | data formatting | bytes 2621440 | tf_op jit(solution)/shard_map/reshape | solution.py:667
  188.7 0.0 copy-start.2
  188.7 0.5 convolution_multiply_fusion.1
  189.2 0.7 copy-done.2
  189.9 1.3 fusion.2
  (4 shorter events, 0.0 us)
Async XLA Ops:
  0.6 152.2 %copy-start = (bf16[256,2048]{1,0:T(8,128)(2,1)S(1)}, bf16[256,2048]{1,0:T(8,128)(2,1)}, u32[]{:S(2)}) copy-start(bf16[256,2048]{1,0:T(8,128)(2,1)} %param.29) | copy-start | bytes 3145732
  145.0 7.8 %copy-start.3 = (bf16[256,256]{1,0:T(8,128)(2,1)S(1)}, bf16[256,256]{1,0:T(8,128)(2,1)}, u32[]{:S(2)}) copy-start(bf16[256,256]{1,0:T(8,128)(2,1)} %get-tuple-element.16) | copy-start | bytes 393220
  145.0 41.3 %all-to-all-start = ((bf16[64,80,128]{2,1,0:T(8,128)(2,1)}), bf16[64,80,128]{2,1,0:T(8,128)(2,1)}, u32[]{:S(2)}, u32[]{:S(2)}) async-start(bf16[64,80,128]{2,1,0:T(8,128)(2,1)} %reshape.52), calls=%async_computation | async-start | bytes 2621440 | tf_op jit(solution)/shard_map/all_to_all | solution.py:654
  153.3 3.7 %copy-start.1 = (bf16[128,2048]{1,0:T(8,128)(2,1)S(1)}, bf16[128,2048]{1,0:T(8,128)(2,1)}, u32[]{:S(2)}) copy-start(bf16[128,2048]{1,0:T(8,128)(2,1)} %expert_ref.1) | copy-start | bytes 1572868
  153.3 3.9 %copy-start.5 = (f32[128,2]{0,1:T(2,128)S(1)}, f32[128,2]{0,1:T(2,128)}, u32[]{:S(2)}) copy-start(f32[128,2]{0,1:T(2,128)} %param.33) | copy-start | bytes 3076
  153.3 3.9 %copy-start.4 = (f32[2048]{0:T(1024)S(1)}, f32[2048]{0:T(1024)}, u32[]{:S(2)}) copy-start(f32[2048]{0:T(1024)} %param.31) | copy-start | bytes 24580
  153.4 13.6 %collective-permute-start.2 = (bf16[64,2048]{1,0:T(8,128)(2,1)S(1)}, bf16[64,2048]{1,0:T(8,128)(2,1)S(1)}, u32[]{:S(2)}, u32[]{:S(2)}) collective-permute-start(bf16[64,2048]{1,0:T(8,128)(2,1)S(1)} %get-tuple-element.25), channel_id=1, source_target_pairs={{0,3},{1,0},{2,1},{3,2},{4,7},{5,4},{6,5},{7,6},{8,11},{9,8},{10,9... | collective-permute-start | bytes 786440 | tf_op jit(solution)/shard_map/ppermute | solution.py:662
  156.3 10.6 %collective-permute-start.1 = (bf16[64,2048]{1,0:T(8,128)(2,1)S(1)}, bf16[64,2048]{1,0:T(8,128)(2,1)S(1)}, u32[]{:S(2)}, u32[]{:S(2)}) collective-permute-start(bf16[64,2048]{1,0:T(8,128)(2,1)S(1)} %get-tuple-element.26), channel_id=1, source_target_pairs={{0,2},{1,3},{2,0},{3,1},{4,6},{5,7},{6,4},{7,5},{8,10},{9,11},{10,... | collective-permute-start | bytes 786440 | tf_op jit(solution)/shard_map/ppermute | solution.py:662
  156.3 14.9 %collective-permute-start = (bf16[64,2048]{1,0:T(8,128)(2,1)S(1)}, bf16[64,2048]{1,0:T(8,128)(2,1)}, u32[]{:S(2)}, u32[]{:S(2)}) collective-permute-start(bf16[64,2048]{1,0:T(8,128)(2,1)S(1)} %get-tuple-element.24), channel_id=1, source_target_pairs={{0,1},{1,2},{2,3},{3,0},{4,5},{5,6},{6,7},{7,4},{8,9},{9,10},{10,1... | collective-permute-start | bytes 786440 | tf_op jit(solution)/shard_map/ppermute | solution.py:662
  188.7 1.2 copy-start.2
